TPU v7x, 32 devices: a whole 2x2x4 slice. The times are simulated.
32 devices in a mesh: sp: 8 (over z, y), tp: 4 (over x, core).
Axes of the slice: x: 2, y: 2, z: 4, core: 2. Of those that a mesh axis runs over, the one named last changes fastest.
Arguments:
- tokens: bfloat16 [8192, 2048], P('sp'), may hold values from -6 to 6
- norm_gain: float32 [2048], replicated, may hold values from 0.1 to 1.9
- w_query: bfloat16 [2048, 1024], P('sp', 'tp'), may hold values from -3.5 to 3.5
- w_key: bfloat16 [2048, 256], P('sp', 'tp'), may hold values from -0.125 to 0.125
- w_value: bfloat16 [2048, 256], P('sp', 'tp'), may hold values from -0.125 to 0.125
- w_content: bfloat16 [2048, 1024], P('sp', 'tp'), may hold values from -0.125 to 0.125
- w_gate: bfloat16 [2048, 1024], P('sp', 'tp'), may hold values from -0.125 to 0.125
- sink_logit: float32 [16], P('tp'), may hold values from 1 to 6
- conv_weight: float32 [31, 1024], P(None, 'tp'), may hold values from -10 to 10
- conv_bias: float32 [1024], P('tp'), may hold values from 0 to 20
- channel_gain: float32 [1024], P('tp'), may hold values from 0.1 to 1.9
- out_attn: bfloat16 [1024, 2048], P('tp', 'sp'), may hold values from -0.75 to 0.75
- out_conv: bfloat16 [1024, 2048], P('tp', 'sp'), may hold values from -0.1875 to 0.1875
Outputs:
- mixed: bfloat16 [8192, 2048], P(('sp', 'tp'))
All inputs are finite; a program needn't handle non-finite values.
Results may differ from a plain program's by a relative error of at most 0.025.
The roundings to bfloat16 on the way count: a program that leaves them out, or rounds other values in their place, can miss the bound.
Values may be sent and summed in bfloat16 or wider, within the bound.
A program may use at most 64 MiB of HBM per device.

v0:
```python
import math

import jax
import jax.numpy as jnp
from jax import lax
from jax.sharding import PartitionSpec as P

HEAD_DIM = 64
CONV_CH = 1024
KERNEL = 31
WINDOW = 128


EPS = 1e-05
THETA = 10000.0


def shifted(block, axis, distance):
    devices = range(lax.axis_size(axis))
    route = [(i - distance, i) for i in devices if i - distance in devices]
    return lax.ppermute(block, axis, route)


def rotate(heads_in, positions):
    half_dim = heads_in.shape[-1] // 2
    inverse = 1.0 / THETA ** (jnp.arange(half_dim, dtype=jnp.float32) * 2.0 / heads_in.shape[-1])
    angles = positions.astype(jnp.float32)[:, None] * inverse[None, :]
    cosine = jnp.cos(angles)[:, None, :]
    sine_part = jnp.sin(angles)[:, None, :]
    former = heads_in[..., :half_dim]
    latter = heads_in[..., half_dim:]
    return jnp.concatenate(
        [former * cosine - latter * sine_part, latter * cosine + former * sine_part], axis=-1
    )


def shards(
    tokens,
    norm_gain,
    w_query,
    w_key,
    w_value,
    w_content,
    w_gate,
    sink_logit,
    conv_weight,
    conv_bias,
    channel_gain,
    out_attn,
    out_conv,
):
    token_count = tokens.shape[0]
    offset = lax.axis_index("sp") * token_count
    positions = offset + jnp.arange(token_count, dtype=jnp.int32)
    tokens_wide = tokens.astype(jnp.float32)
    inv_rms = lax.rsqrt(jnp.mean(tokens_wide * tokens_wide, axis=1, keepdims=True) + EPS)
    scaled = (tokens_wide * norm_gain[None, :]).astype(jnp.bfloat16)
    widths = [
        w_query.shape[1],
        w_key.shape[1],
        w_value.shape[1],
        w_content.shape[1],
        w_gate.shape[1],
    ]
    whole_weights = (
        lax.all_gather(w_query, "sp", axis=0, tiled=True),
        lax.all_gather(w_key, "sp", axis=0, tiled=True),
        lax.all_gather(w_value, "sp", axis=0, tiled=True),
        lax.all_gather(w_content, "sp", axis=0, tiled=True),
        lax.all_gather(w_gate, "sp", axis=0, tiled=True),
    )
    joined_whole = jnp.concatenate(whole_weights, axis=1)
    projected = jnp.dot(scaled, joined_whole, preferred_element_type=jnp.float32)
    projected = projected * inv_rms
    bounds = [0]
    for width in widths:
        bounds.append(bounds[-1] + width)
    proj_query = projected[:, bounds[0] : bounds[1]]
    proj_key = projected[:, bounds[1] : bounds[2]]
    proj_value = projected[:, bounds[2] : bounds[3]]
    proj_content = projected[:, bounds[3] : bounds[4]]
    proj_gate = projected[:, bounds[4] : bounds[5]]
    kv_local = widths[1] // HEAD_DIM
    heads_local = widths[0] // HEAD_DIM
    group_size = heads_local // kv_local
    queries = rotate(proj_query.reshape(token_count, heads_local, HEAD_DIM), positions).astype(
        jnp.bfloat16
    )
    key_rows = rotate(proj_key.reshape(token_count, kv_local, HEAD_DIM), positions).astype(
        jnp.bfloat16
    )
    value_rows = proj_value.astype(jnp.bfloat16).reshape(token_count, kv_local, HEAD_DIM)
    glu_out = (proj_content * jax.nn.sigmoid(proj_gate)).astype(jnp.bfloat16)
    prior_key, prior_value, prior_glu = shifted(
        (
            key_rows[token_count - WINDOW :],
            value_rows[token_count - WINDOW :],
            glu_out[token_count - (KERNEL - 1) :],
        ),
        "sp",
        1,
    )
    key_ext = jnp.concatenate([prior_key, key_rows], 0)
    value_ext = jnp.concatenate([prior_value, value_rows], 0)
    block_rows = math.gcd(token_count, 512)
    sink_col = sink_logit.reshape(kv_local, group_size)[:, :, None, None]

    def attend(block_start):
        query_blk = lax.dynamic_slice_in_dim(queries, block_start, block_rows, 0).reshape(
            block_rows, kv_local, group_size, HEAD_DIM
        )
        key_blk = lax.dynamic_slice_in_dim(key_ext, block_start, block_rows + WINDOW, 0)
        value_blk = lax.dynamic_slice_in_dim(value_ext, block_start, block_rows + WINDOW, 0)
        scores = jnp.einsum(
            "qkgd,jkd->kgqj", query_blk, key_blk, preferred_element_type=jnp.float32
        ) * HEAD_DIM ** (-0.5)
        query_pos = offset + block_start + jnp.arange(block_rows, dtype=jnp.int32)
        key_pos = offset + block_start - WINDOW + jnp.arange(block_rows + WINDOW, dtype=jnp.int32)
        distance = query_pos[:, None] - key_pos[None, :]
        allowed = (distance >= 0) & (distance < WINDOW) & (key_pos[None, :] >= 0)
        scores = jnp.where(allowed[None, None], scores, -1e30)
        row_max = jnp.maximum(jnp.max(scores, axis=-1, keepdims=True), sink_col)
        weights = jnp.exp(scores - row_max)
        denominator = jnp.sum(weights, axis=-1, keepdims=True) + jnp.exp(sink_col - row_max)
        probability = (weights / denominator).astype(jnp.bfloat16)
        attended = jnp.einsum(
            "kgqj,jkd->qkgd", probability, value_blk, preferred_element_type=jnp.float32
        )
        return attended.reshape(block_rows, heads_local * HEAD_DIM).astype(jnp.bfloat16)

    starts = jnp.arange(0, token_count, block_rows, dtype=jnp.int32)
    attn_out = lax.map(attend, starts).reshape(token_count, heads_local * HEAD_DIM)
    padded = jnp.concatenate([prior_glu, glu_out], 0)
    conv_sum = jnp.zeros(glu_out.shape, jnp.float32) + conv_bias[None, :]
    for tap_index in range(KERNEL):
        window_rows = lax.slice_in_dim(padded, tap_index, tap_index + token_count, axis=0)
        conv_sum = conv_sum + conv_weight[tap_index][None, :] * window_rows.astype(jnp.float32)
    row_sum, row_squares = lax.psum(
        (jnp.sum(conv_sum, axis=1), jnp.sum(conv_sum * conv_sum, axis=1)), "tp"
    )
    centre = row_sum / CONV_CH
    variance = jnp.maximum(row_squares / CONV_CH - centre * centre, 0.0)
    centred = conv_sum - centre[:, None]
    conv_out = jax.nn.silu(
        centred * lax.rsqrt(variance + EPS)[:, None] * channel_gain[None, :]
    ).astype(jnp.bfloat16)
    attn_weight, conv_weight_out = (
        lax.all_gather(out_attn, "sp", axis=1, tiled=True),
        lax.all_gather(out_conv, "sp", axis=1, tiled=True),
    )
    return lax.psum_scatter(
        (
            jnp.dot(attn_out, attn_weight, preferred_element_type=jnp.float32)
            + jnp.dot(conv_out, conv_weight_out, preferred_element_type=jnp.float32)
        ).astype(jnp.bfloat16),
        "tp",
        scatter_dimension=0,
        tiled=True,
    )


def solution(mesh):
    placed = (
        P("sp", None),
        P(),
        P("sp", "tp"),
        P("sp", "tp"),
        P("sp", "tp"),
        P("sp", "tp"),
        P("sp", "tp"),
        P("tp"),
        P(None, "tp"),
        P("tp"),
        P("tp"),
        P("tp", "sp"),
        P("tp", "sp"),
    )
    return jax.shard_map(
        shards, mesh=mesh, in_specs=placed, out_specs=P(("sp", "tp"), None), check_vma=False
    )
```

profile of v0, /device:TPU:0, one launch (start us, length us, event | category | flops | bytes accessed | tf_op | source)
XLA Modules:
  0.0 276.7 jit_solution(9602372100434839561)
XLA Ops:
  12.0 3.1 %fusion.20 = f32[1024]{0:T(1024)S(1)} fusion(bf16[1024,2048]{1,0:T(8,128)(2,1)} %param.15), kind=kLoop, calls=%fused_computation.31 | loop fusion | flops 6290432 | bytes 4198400 | tf_op jit(solution)/shard_map/reduce_sum | solution.py:56
  16.9 33.8 %all_gather.23 = bf16[2048,64]{1,0:T(8,128)(2,1)S(1)} all-gather(bf16[256,64]{1,0:T(8,128)(2,1)S(1)} %copy.19), channel_id=1, replica_groups=mesh['sp'=8,'tp'=4] {'sp'}, dimensions={0}, use_global_device_ids=true | all-gather | bytes 294912 | tf_op jit(solution)/shard_map/all_gather | solution.py:68
  50.6 31.7 %all_gather.22 = bf16[2048,64]{1,0:T(8,128)(2,1)S(1)} all-gather(bf16[256,64]{1,0:T(8,128)(2,1)S(1)} %copy.18), channel_id=1, replica_groups=mesh['sp'=8,'tp'=4] {'sp'}, dimensions={0}, use_global_device_ids=true | all-gather | bytes 294912 | tf_op jit(solution)/shard_map/all_gather | solution.py:67
  83.0 14.4 %all-gather.8.cloned.1.call-done = bf16[2048,256]{1,0:T(8,128)(2,1)} async-done(((bf16[256,256]{1,0:T(8,128)(2,1)}), bf16[2048,256]{1,0:T(8,128)(2,1)}) %all-gather.8.cloned.1.call-update) | async-done | bytes 1048592 | tf_op jit(solution)/shard_map/all_gather | solution.py:69
  97.4 41.2 %all-gather.10.cloned.1.call-done = bf16[2048,256]{1,0:T(8,128)(2,1)} async-done(((bf16[256,256]{1,0:T(8,128)(2,1)}), bf16[2048,256]{1,0:T(8,128)(2,1)}) %all-gather.10.cloned.1.call-update) | async-done | bytes 1048592 | tf_op jit(solution)/shard_map/all_gather | solution.py:70
  138.5 6.7 %concatenate.28 = bf16[2048,896]{1,0:T(8,128)(2,1)} concatenate(bf16[2048,256]{1,0:T(8,128)(2,1)} %all-gather.6.cloned.1.call-done, bf16[2048,64]{1,0:T(8,128)(2,1)S(1)} %all_gather.22, bf16[2048,64]{1,0:T(8,128)(2,1)S(1)} %all_gather.23, bf16[2048,256]{1,0:T(8,128)(2,1)} %all-gather.8.cloned.1.call-done, bf16[2048,256]{1,0:T(8,128)(2,1)} %all-gather.10.cloned.1.call-done), dimensions={1} | concatenate | bytes 7340032 | tf_op jit(solution)/shard_map/concatenate | solution.py:72
  145.2 7.0 %fusion.77 = (bf16[1024,896]{0,1:T(8,128)(2,1)S(1)}, f32[1024,896]{0,1:T(8,128)S(1)}) fusion(f32[1024]{0:T(1024)S(1)} %add_rsqrt_fusion.1, bf16[2048,896]{1,0:T(8,128)(2,1)} %concatenate.28, bf16[1024,2048]{1,0:T(8,128)(2,1)} %param.15, f32[2048]{0:T(1024)S(1)} %copy-done.3), kind=kOutput, calls=%fused_computation.147 | convolution fusion | flops 3766222848 | bytes 13381632 | tf_op jit(solution)/shard_map/dot_general | solution.py:73
  152.6 2.4 collective-permute-start
  155.6 3.1 %collective-permute-start.1 = (bf16[128,1,64]{0,2,1:T(8,128)(2,1)S(1)}, bf16[128,1,64]{0,2,1:T(8,128)(2,1)S(1)}, u32[]{:S(2)}, u32[]{:S(2)}) collective-permute-start(bf16[128,1,64]{0,2,1:T(8,128)(2,1)S(1)} %pad_maximum_fusion.3), channel_id=1, source_target_pairs={{0,4},{4,8},{8,12},{12,16},{16,20},{20,24},{24,28},{1,5},{5,9},{9,... | collective-permute-start | bytes 49160 | tf_op jit(solution)/shard_map/ppermute | solution.py:21
  158.8 2.5 collective-permute-start.2
  161.6 1.7 collective-permute-done.2
  163.3 7.8 %fusion.74 = (f32[1024]{0:T(1024)S(1)}, f32[1024]{0:T(1024)S(1)}, f32[1024,256]{0,1:T(8,128)S(1)}) fusion(bf16[1024,256]{0,1:T(8,128)(2,1)S(1)} %get-tuple-element.130, f32[256]{0:T(256)S(1)} %bitcast.115, bf16[30,256]{0,1:T(8,128)(2,1)S(1)} %collective-permute-done.2, f32[256]{0:T(256)S(1)} %bitcast.116, f32[256]{0:T(256)S(1)} %bitcast.118, ...), kind=kLoop, calls=%fused_computation.144 | loop fusion | flops 48756736 | bytes 1629184 | tf_op jit(solution)/shard_map/reduce_sum | solution.py:139
  171.1 6.1 %all-reduce = (f32[1024]{0:T(1024)S(1)}, f32[1024]{0:T(1024)S(1)}) all-reduce(f32[1024]{0:T(1024)S(1)} %get-tuple-element.108, f32[1024]{0:T(1024)S(1)} %get-tuple-element.107), channel_id=1, replica_groups=mesh['sp'=8,'tp'=4] {'tp'}, use_global_device_ids=true, to_apply=%region_8.9 | all-reduce | flops 2048 | bytes 16384 | tf_op jit(solution)/shard_map/psum | solution.py:138
  177.3 18.4 %while.12 = (s32[]{:T(128)}, bf16[2,512,256]{2,1,0:T(8,128)(2,1)S(1)}, s32[2]{0:T(128)S(1)}, bf16[1152,1,64]{0,2,1:T(8,128)(2,1)S(1)}, s32[]{:T(128)}, /*index=5...) while((s32[]{:T(128)}, ...), condition=%wide.region_4.5_spmd, body=%wide.region_1.4_spmd.sunk | while | flops 353048960 | bytes 18868768 | solution.py:132
  182.1 1.2 fusion.92
  183.4 1.1 fusion.93
  184.6 1.7 fusion.94
  191.3 1.2 fusion.92
  192.6 1.1 fusion.93
  193.8 1.7 fusion.94
  195.7 5.7 %fusion.78 = f32[1024,2048]{1,0:T(8,128)} fusion(bf16[1024,256]{1,0:T(8,128)(2,1)S(1)} %bitcast.101, bf16[256,2048]{1,0:T(8,128)(2,1)} %all-gather.12.cloned.1.call-done), kind=kOutput, calls=%fused_computation.148 | convolution fusion | flops 1073741824 | bytes 9961472 | tf_op jit(solution)/shard_map/dot_general | solution.py:153
  201.5 17.5 %all-gather.14.cloned.1.call-done = bf16[256,2048]{1,0:T(8,128)(2,1)} async-done(((bf16[256,256]{1,0:T(8,128)(2,1)}), bf16[256,2048]{1,0:T(8,128)(2,1)}) %all-gather.14.cloned.1.call-update) | async-done | bytes 1048592 | tf_op jit(solution)/shard_map/all_gather | solution.py:149
  218.9 7.2 %add_convert_fusion = bf16[1024,2048]{1,0:T(8,128)(2,1)} fusion(f32[1024,2048]{1,0:T(8,128)} %fusion.78, bf16[256,2048]{1,0:T(8,128)(2,1)} %all-gather.14.cloned.1.call-done, f32[1024,256]{0,1:T(8,128)S(1)} %get-tuple-element.127, f32[256]{0:T(256)S(1)} %copy-done.2, f32[1024]{0:T(1024)S(1)} %get-tuple-element.170, f32[1024]{0:T(1024)S(1)} %get-tuple-element.169), kind=kOutput, calls=%fused_computation.32 | convolution fusion | flops 1080033280 | bytes 14689280 | tf_op jit(solution)/shard_map/dot_general | solution.py:154
  226.1 43.7 %reduce-scatter.2.cloned.1.call-done = bf16[256,2048]{1,0:T(8,128)(2,1)} async-done(((bf16[1024,2048]{1,0:T(8,128)(2,1)}), bf16[256,2048]{1,0:T(8,128)(2,1)}) %reduce-scatter.2.cloned.1.call-update) | async-done | bytes 1048592 | tf_op jit(solution)/shard_map/reduce_scatter | solution.py:151
  (64 shorter events, 11.7 us)
Async XLA Ops:
  6.5 76.4 %all-gather.6.cloned.1.call-start = ((), (), s32[]{:S(2)}) async-start(), calls=%async_computation.1 | async-start | bytes 1179648 | tf_op jit(solution)/shard_map/all_gather | solution.py:66
  7.3 90.1 %all-gather.8.cloned.1.call-start = ((), (), s32[]{:S(2)}) async-start(), calls=%async_computation.2 | async-start | bytes 1179648 | tf_op jit(solution)/shard_map/all_gather | solution.py:69
  8.0 130.5 %all-gather.10.cloned.1.call-start = ((), (), s32[]{:S(2)}) async-start(), calls=%async_computation.3 | async-start | bytes 1179648 | tf_op jit(solution)/shard_map/all_gather | solution.py:70
  8.7 187.0 %all-gather.12.cloned.1.call-start = ((), (), s32[]{:S(2)}) async-start(), calls=%async_computation.4 | async-start | bytes 1179648 | tf_op jit(solution)/shard_map/all_gather | solution.py:148
  9.3 209.6 %all-gather.14.cloned.1.call-start = ((), (), s32[]{:S(2)}) async-start(), calls=%async_computation.5 | async-start | bytes 1179648 | tf_op jit(solution)/shard_map/all_gather | solution.py:149
  9.9 260.0 %reduce-scatter.2.cloned.1.call-start = ((), (), s32[]{:S(2)}) async-start(), calls=%async_computation.6 | async-start | bytes 5242880 | tf_op jit(solution)/shard_map/reduce_scatter | solution.py:151
  15.1 130.1 %copy-start.3 = (f32[2048]{0:T(1024)S(1)}, f32[2048]{0:T(1024)}, u32[]{:S(2)}) copy-start(f32[2048]{0:T(1024)} %param.16) | copy-start | bytes 24580
  152.2 11.0 %copy-start.1 = (f32[256]{0:T(256)S(1)}, f32[256]{0:T(256)}, u32[]{:S(2)}) copy-start(f32[256]{0:T(256)} %param.24) | copy-start | bytes 3076
  152.3 25.0 %copy-start = (f32[4]{0:T(128)S(1)}, f32[4]{0:T(128)}, u32[]{:S(2)}) copy-start(f32[4]{0:T(128)} %param.22) | copy-start | bytes 52
  152.6 24.6 %collective-permute-start = (bf16[128,1,64]{0,2,1:T(8,128)(2,1)S(1)}, bf16[128,1,64]{0,2,1:T(8,128)(2,1)S(1)}, u32[]{:S(2)}, u32[]{:S(2)}) collective-permute-start(bf16[128,1,64]{0,2,1:T(8,128)(2,1)S(1)} %slice_bitcast_fusion.2), channel_id=1, source_target_pairs={{0,4},{4,8},{8,12},{12,16},{16,20},{20,24},{24,28},{1,5},{5,9},{9,... | collective-permute-start | bytes 49160 | tf_op jit(solution)/shard_map/ppermute | solution.py:21
  155.6 21.6 %collective-permute-start.1 = (bf16[128,1,64]{0,2,1:T(8,128)(2,1)S(1)}, bf16[128,1,64]{0,2,1:T(8,128)(2,1)S(1)}, u32[]{:S(2)}, u32[]{:S(2)}) collective-permute-start(bf16[128,1,64]{0,2,1:T(8,128)(2,1)S(1)} %pad_maximum_fusion.3), channel_id=1, source_target_pairs={{0,4},{4,8},{8,12},{12,16},{16,20},{20,24},{24,28},{1,5},{5,9},{9,... | collective-permute-start | bytes 49160 | tf_op jit(solution)/shard_map/ppermute | solution.py:21
  158.8 4.4 %collective-permute-start.2 = (bf16[30,256]{0,1:T(8,128)(2,1)S(1)}, bf16[30,256]{0,1:T(8,128)(2,1)S(1)}, u32[]{:S(2)}, u32[]{:S(2)}) collective-permute-start(bf16[30,256]{0,1:T(8,128)(2,1)S(1)} %slice.308), channel_id=1, source_target_pairs={{0,4},{4,8},{8,12},{12,16},{16,20},{20,24},{24,28},{1,5},{5,9},{9,... | collective-permute-start | bytes 46088 | tf_op jit(solution)/shard_map/ppermute | solution.py:21
  195.7 23.2 %copy-start.2 = (f32[256]{0:T(256)S(1)}, f32[256]{0:T(256)}, u32[]{:S(2)}) copy-start(f32[256]{0:T(256)} %param.25) | copy-start | bytes 3076
Sparse Core Ops, SparseCore 0:
  9.5 45.0 all-gather.5
  56.6 40.6 all-gather.7
  99.5 38.9 all-gather.9
  140.4 38.1 all-gather.11
  180.5 38.3 all-gather.13
  226.3 43.5 reduce-scatter.1
where the time goes:
time: 278 us; the launch traced here: 277 us
  waiting for transfers between devices  122 us (44%)
  blocking collectives  71.6 us (26%)
  matrix products  25.7 us (9%)
  other arithmetic  15.9 us (6%)
  between operations  13.7 us (5%)
  local copies, waits for them, and re-layouts  12.2 us (4%)
  starting transfers between devices  8.25 us (3%)
  loops' own time  7.56 us (3%)
    reduce_scatter x1, waiting for transfers between devices, shards(): lax.psum_scatter((jnp.dot(attn_out, attn_weight, preferred_element_type=j...  43.7 us
    all_gather x1, waiting for transfers between devices, shards(): lax.all_gather(w_gate, 'sp', axis=0, tiled=True)  41.2 us
    all_gather x1, blocking collectives, shards(): lax.all_gather(w_value, 'sp', axis=0, tiled=True)  33.8 us
    all_gather x1, blocking collectives, shards(): lax.all_gather(w_key, 'sp', axis=0, tiled=True)  31.7 us
    all_gather x1, waiting for transfers between devices, shards(): lax.all_gather(out_conv, 'sp', axis=1, tiled=True)  17.5 us
    all_gather x1, waiting for transfers between devices, shards(): lax.all_gather(w_content, 'sp', axis=0, tiled=True)  14.4 us
    ppermute x3, starting transfers between devices, shifted(): return lax.ppermute(block, axis, route)  8.06 us
    reduce_sum x1, other arithmetic, shards(): jnp.sum(conv_sum, axis=1)  7.81 us
  transfers between devices with their start and end apart: 9, of which 5 were waited for; matrix products, arithmetic and copies ran while one was open for 17% of the time, Pallas kernels for 0%

commit v1 on v0

--- a/solution.py
+++ b/solution.py
@@ -1,8 +1,11 @@
+import functools
 import math
 
 import jax
 import jax.numpy as jnp
 from jax import lax
+from jax.experimental import pallas as pl
+from jax.experimental.pallas import tpu as pltpu
 from jax.sharding import PartitionSpec as P
 
 HEAD_DIM = 64
@@ -34,7 +37,245 @@
     )
 
 
-def shards(
+MESH = pl.DeviceIdType.MESH
+LANES = 128
+VMEM_GRANT = 60 * 1024 * 1024
+
+
+def ring_place(index, n):
+    odd = index % 2
+    return (index // 2) * (1 - odd) + (n - 1 - index // 2) * odd
+
+
+def ring_member(place, n):
+    return jnp.where(place < (n + 1) // 2, 2 * place, 2 * (n - 1 - place) + 1)
+
+
+def greet(peers):
+    barrier = pltpu.get_barrier_semaphore()
+    for peer in peers:
+        pl.semaphore_signal(barrier, inc=1, device_id=peer, device_id_type=MESH)
+    pl.semaphore_wait(barrier, len(peers))
+
+
+def project_kernel(
+    n, pieces, tok_ref, gain_ref, w_ref, o_ref, proj_ref, og_ref,
+    scaled, inv, wg, w_send, w_recv, o_send, o_recv,
+):
+    me = lax.axis_index("sp")
+    place = ring_place(me, n)
+    after = {"sp": ring_member(lax.rem(place + 1, n), n)}
+    before = {"sp": ring_member(lax.rem(place + n - 1, n), n)}
+    greet((after, before))
+
+    def hop(own, held, send, recv, d, c, s):
+        half = own.shape[0] // 2
+        sub = half // pieces
+        rows = pl.ds(d * half + c * sub, sub)
+        offset = n - s if d == 0 else s
+        owner = ring_member(lax.rem(place + offset, n), n)
+        return pltpu.make_async_remote_copy(
+            src_ref=own.at[rows] if s == 0 else held.at[owner, rows],
+            dst_ref=held.at[owner, rows],
+            send_sem=send.at[d, s, c],
+            recv_sem=recv.at[d, s, c],
+            device_id=after if d == 0 else before,
+            device_id_type=MESH,
+        )
+
+    def w_hop(d, c, s):
+        return hop(w_ref, wg, w_send, w_recv, d, c, s)
+
+    def o_hop(d, c, s):
+        return hop(o_ref, og_ref, o_send, o_recv, d, c, s)
+
+    lanes = [(d, c) for c in range(pieces) for d in range(2)]
+    for d, c in lanes:
+        w_hop(d, c, 0).start()
+    for d, c in lanes:
+        o_hop(d, c, 0).start()
+
+    token_count, width = tok_ref.shape
+    depth = w_ref.shape[0]
+    step_rows = math.gcd(token_count, 64)
+
+    @pl.loop(0, token_count // step_rows)
+    def _(i):
+        rows = pl.ds(pl.multiple_of(i * step_rows, step_rows), step_rows)
+        wide = tok_ref[rows, :].astype(jnp.float32)
+        inv[rows, :] = lax.rsqrt(jnp.sum(wide * wide, axis=1, keepdims=True) / width + EPS)
+        scaled[rows, :] = (wide * gain_ref[...]).astype(jnp.bfloat16)
+
+    tile = math.gcd(token_count, 256)
+    og_ref[me] = o_ref[...]
+
+    def add(terms, first, last):
+        @pl.loop(0, token_count // tile)
+        def _(i):
+            rows = pl.ds(pl.multiple_of(i * tile, tile), tile)
+            total = None if first else proj_ref[rows, :]
+            for owner, block in terms:
+                columns = pl.ds(pl.multiple_of(owner * depth, depth), depth)
+                term = jnp.dot(
+                    scaled[rows, columns], block(), preferred_element_type=jnp.float32
+                )
+                total = term if total is None else total + term
+            proj_ref[rows, :] = total * inv[rows, :] if last else total
+
+    add([(me, lambda: w_ref[...])], True, n == 1)
+    for t in range(n - 1):
+        for d, c in lanes:
+            w_hop(d, c, t).wait_recv()
+            if t < n - 2:
+                w_hop(d, c, t + 1).start()
+        for d, c in lanes:
+            o_hop(d, c, t).wait_recv()
+            if t < n - 2:
+                o_hop(d, c, t + 1).start()
+        ready = [k for k in range(1, n) if max(k, n - k) - 1 == t]
+        if ready:
+            owners = [ring_member(lax.rem(place + n - k, n), n) for k in ready]
+            add([(o, lambda o=o: wg[o]) for o in owners], False, t == n - 2)
+    for t in range(n - 1):
+        for d, c in lanes:
+            w_hop(d, c, t).wait_send()
+            o_hop(d, c, t).wait_send()
+
+
+def gather_and_project(n, tokens, gain, w_own, o_own):
+    token_count = tokens.shape[0]
+    width = w_own.shape[1]
+    pieces = 2
+    sems = pltpu.SemaphoreType.DMA((2, n - 1, pieces))
+    vmem = pl.BlockSpec(memory_space=pltpu.VMEM)
+    return pl.pallas_call(
+        functools.partial(project_kernel, n, pieces),
+        out_shape=(
+            jax.ShapeDtypeStruct((token_count, width), jnp.float32),
+            jax.ShapeDtypeStruct((n,) + o_own.shape, jnp.bfloat16),
+        ),
+        in_specs=[vmem] * 4,
+        out_specs=(vmem, vmem),
+        scratch_shapes=[
+            pltpu.VMEM(tokens.shape, jnp.bfloat16),
+            pltpu.VMEM((token_count, 1), jnp.float32),
+            pltpu.VMEM((n,) + w_own.shape, jnp.bfloat16),
+            sems, sems, sems, sems,
+        ],
+        compiler_params=pltpu.CompilerParams(
+            collective_id=0, has_side_effects=True, vmem_limit_bytes=VMEM_GRANT
+        ),
+        name="gather_project",
+    )(tokens, gain[None, :], w_own, o_own)
+
+
+def mix_kernel(
+    parts, act_ref, og_ref, out_ref, near_out, near_in, far_out, far_in,
+    near_send, near_recv, far_send, far_recv,
+):
+    me = lax.axis_index("tp")
+    core = me % 2
+    near = me + 1 - 2 * core
+    far = lax.rem(me + 2, 4)
+    far_near = lax.rem(near + 2, 4)
+    near_id, far_id = {"tp": near}, {"tp": far}
+    greet((near_id, far_id))
+    rows_out = out_ref.shape[0]
+    blocks = og_ref.shape[0] // parts
+    cols = og_ref.shape[2]
+
+    def partial_of(member, q):
+        rows = pl.ds(pl.multiple_of(member * rows_out, rows_out), rows_out)
+        acts = act_ref[rows, :]
+        return jnp.concatenate(
+            [
+                jnp.dot(acts, og_ref[q * blocks + b], preferred_element_type=jnp.float32)
+                for b in range(blocks)
+            ],
+            axis=1,
+        )
+
+    def near_copy(which, q):
+        return pltpu.make_async_remote_copy(
+            src_ref=near_out.at[which, q],
+            dst_ref=near_in.at[which, q],
+            send_sem=near_send.at[which, q],
+            recv_sem=near_recv.at[which, q],
+            device_id=near_id,
+            device_id_type=MESH,
+        )
+
+    def far_copy(q):
+        return pltpu.make_async_remote_copy(
+            src_ref=far_out.at[q],
+            dst_ref=far_in.at[q],
+            send_sem=far_send.at[q],
+            recv_sem=far_recv.at[q],
+            device_id=far_id,
+            device_id_type=MESH,
+        )
+
+    def give_near(which, member, q):
+        near_out[which, q] = partial_of(member, q).astype(jnp.bfloat16)
+        near_copy(which, q).start()
+
+    def give_far(q):
+        mine = partial_of(far, q)
+        near_copy(0, q).wait_recv()
+        far_out[q] = (mine + near_in[0, q].astype(jnp.float32)).astype(jnp.bfloat16)
+        far_copy(q).start()
+
+    give_near(0, far_near, 0)
+    for q in range(1, parts):
+        give_near(0, far_near, q)
+        give_far(q - 1)
+    give_far(parts - 1)
+    for q in range(parts):
+        give_near(1, near, q)
+    for q in range(parts):
+        mine = partial_of(me, q)
+        near_copy(1, q).wait_recv()
+        mine = mine + near_in[1, q].astype(jnp.float32)
+        far_copy(q).wait_recv()
+        span = blocks * cols
+        out_ref[:, q * span : (q + 1) * span] = (
+            mine + far_in[q].astype(jnp.float32)
+        ).astype(jnp.bfloat16)
+    for q in range(parts):
+        near_copy(0, q).wait_send()
+        near_copy(1, q).wait_send()
+        far_copy(q).wait_send()
+
+
+def mix_and_scatter(acts, og):
+    n, _, cols = og.shape
+    parts = math.gcd(n, 4)
+    rows_out = acts.shape[0] // 4
+    span = n // parts * cols
+    vmem = pl.BlockSpec(memory_space=pltpu.VMEM)
+    return pl.pallas_call(
+        functools.partial(mix_kernel, parts),
+        out_shape=jax.ShapeDtypeStruct((rows_out, n * cols), jnp.bfloat16),
+        in_specs=[vmem] * 2,
+        out_specs=vmem,
+        scratch_shapes=[
+            pltpu.VMEM((2, parts, rows_out, span), jnp.bfloat16),
+            pltpu.VMEM((2, parts, rows_out, span), jnp.bfloat16),
+            pltpu.VMEM((parts, rows_out, span), jnp.bfloat16),
+            pltpu.VMEM((parts, rows_out, span), jnp.bfloat16),
+            pltpu.SemaphoreType.DMA((2, parts)),
+            pltpu.SemaphoreType.DMA((2, parts)),
+            pltpu.SemaphoreType.DMA((parts,)),
+            pltpu.SemaphoreType.DMA((parts,)),
+        ],
+        compiler_params=pltpu.CompilerParams(
+            collective_id=1, has_side_effects=True, vmem_limit_bytes=VMEM_GRANT
+        ),
+        name="mix_scatter",
+    )(acts, og)
+
+
+def plain_shards(
     tokens,
     norm_gain,
     w_query,
@@ -159,6 +400,108 @@
     )
 
 
+def ring_shards(
+    tokens,
+    norm_gain,
+    w_query,
+    w_key,
+    w_value,
+    w_content,
+    w_gate,
+    sink_logit,
+    conv_weight,
+    conv_bias,
+    channel_gain,
+    out_attn,
+    out_conv,
+):
+    token_count = tokens.shape[0]
+    offset = lax.axis_index("sp") * token_count
+    positions = offset + jnp.arange(token_count, dtype=jnp.int32)
+    widths = [
+        w_query.shape[1],
+        w_key.shape[1],
+        w_value.shape[1],
+        w_content.shape[1],
+        w_gate.shape[1],
+    ]
+    w_own = jnp.concatenate([w_query, w_key, w_value, w_content, w_gate], axis=1)
+    o_own = jnp.concatenate([out_attn, out_conv], axis=0)
+    projected, mix_weight = gather_and_project(
+        lax.axis_size("sp"), tokens, norm_gain, w_own, o_own
+    )
+    bounds = [0]
+    for width in widths:
+        bounds.append(bounds[-1] + width)
+    proj_query = projected[:, bounds[0] : bounds[1]]
+    proj_key = projected[:, bounds[1] : bounds[2]]
+    proj_value = projected[:, bounds[2] : bounds[3]]
+    proj_content = projected[:, bounds[3] : bounds[4]]
+    proj_gate = projected[:, bounds[4] : bounds[5]]
+    kv_local = widths[1] // HEAD_DIM
+    heads_local = widths[0] // HEAD_DIM
+    group_size = heads_local // kv_local
+    queries = rotate(proj_query.reshape(token_count, heads_local, HEAD_DIM), positions).astype(
+        jnp.bfloat16
+    )
+    key_rows = rotate(proj_key.reshape(token_count, kv_local, HEAD_DIM), positions).astype(
+        jnp.bfloat16
+    )
+    value_rows = proj_value.astype(jnp.bfloat16).reshape(token_count, kv_local, HEAD_DIM)
+    glu_out = (proj_content * jax.nn.sigmoid(proj_gate)).astype(jnp.bfloat16)
+    prior_key, prior_value, prior_glu = shifted(
+        (
+            key_rows[token_count - WINDOW :],
+            value_rows[token_count - WINDOW :],
+            glu_out[token_count - (KERNEL - 1) :],
+        ),
+        "sp",
+        1,
+    )
+    key_ext = jnp.concatenate([prior_key, key_rows], 0)
+    value_ext = jnp.concatenate([prior_value, value_rows], 0)
+    blocks = token_count // WINDOW
+    sink_col = sink_logit.reshape(kv_local, group_size)[None, :, :, None, None]
+    query_blk = queries.reshape(blocks, WINDOW, kv_local, group_size, HEAD_DIM)
+
+    def windows(ext):
+        cut = ext.reshape(blocks + 1, WINDOW, kv_local, HEAD_DIM)
+        return jnp.concatenate([cut[:-1], cut[1:]], axis=1)
+
+    scores = jnp.einsum(
+        "bqkgd,bjkd->bkgqj", query_blk, windows(key_ext), preferred_element_type=jnp.float32
+    ) * HEAD_DIM ** (-0.5)
+    query_off = jnp.arange(WINDOW, dtype=jnp.int32)
+    key_off = jnp.arange(2 * WINDOW, dtype=jnp.int32) - WINDOW
+    distance = query_off[:, None] - key_off[None, :]
+    key_pos = offset + jnp.arange(blocks, dtype=jnp.int32)[:, None] * WINDOW + key_off[None, :]
+    allowed = ((distance >= 0) & (distance < WINDOW))[None] & (key_pos >= 0)[:, None, :]
+    scores = jnp.where(allowed[:, None, None], scores, -1e30)
+    row_max = jnp.maximum(jnp.max(scores, axis=-1, keepdims=True), sink_col)
+    weights = jnp.exp(scores - row_max)
+    denominator = jnp.sum(weights, axis=-1, keepdims=True) + jnp.exp(sink_col - row_max)
+    probability = (weights / denominator).astype(jnp.bfloat16)
+    attended = jnp.einsum(
+        "bkgqj,bjkd->bqkgd", probability, windows(value_ext), preferred_element_type=jnp.float32
+    )
+    attn_out = attended.reshape(token_count, heads_local * HEAD_DIM).astype(jnp.bfloat16)
+    padded = jnp.concatenate([prior_glu, glu_out], 0)
+    conv_sum = jnp.zeros(glu_out.shape, jnp.float32) + conv_bias[None, :]
+    for tap_index in range(KERNEL):
+        window_rows = lax.slice_in_dim(padded, tap_index, tap_index + token_count, axis=0)
+        conv_sum = conv_sum + conv_weight[tap_index][None, :] * window_rows.astype(jnp.float32)
+    row_sum, row_squares = lax.psum(
+        (jnp.sum(conv_sum, axis=1), jnp.sum(conv_sum * conv_sum, axis=1)), "tp"
+    )
+    centre = row_sum / CONV_CH
+    variance = jnp.maximum(row_squares / CONV_CH - centre * centre, 0.0)
+    centred = conv_sum - centre[:, None]
+    conv_out = jax.nn.silu(
+        centred * lax.rsqrt(variance + EPS)[:, None] * channel_gain[None, :]
+    ).astype(jnp.bfloat16)
+    return mix_and_scatter(jnp.concatenate([attn_out, conv_out], axis=1), mix_weight)
+
+
 def solution(mesh):
     placed = (
         P("sp", None),
@@ -175,6 +518,18 @@
         P("tp", "sp"),
         P("tp", "sp"),
     )
+    sp, tp = mesh.shape["sp"], mesh.shape["tp"]
+    ringed = tp == 4 and sp % 2 == 0
+
+    def shards(*arrays):
+        fits = (
+            ringed
+            and arrays[11].shape[1] % LANES == 0
+            and arrays[2].shape[0] % LANES == 0
+            and arrays[0].shape[0] % (WINDOW * tp) == 0
+        )
+        return (ring_shards if fits else plain_shards)(*arrays)
+
     return jax.shard_map(
         shards, mesh=mesh, in_specs=placed, out_specs=P(("sp", "tp"), None), check_vma=False
     )

time: 278 us -> 159 us (0.57)
  waiting for transfers between devices: 122 us -> 0.01 us
  Pallas kernels: 0 us -> 97.3 us
  blocking collectives: 71.6 us -> 5.95 us
  matrix products: 25.7 us -> 3.09 us
  between operations: 13.7 us -> 0.24 us
  other arithmetic: 15.9 us -> 24.1 us
  loops' own time: 7.56 us -> 0 us
  local copies, waits for them, and re-layouts: 12.2 us -> 16.4 us
    pallas_call x0 -> x2, Pallas kernels: none -> 97.3 us  [the longest x1 66.8 us: gather_and_project(): pl.pallas_call(functools.partial(project_kernel, n, pieces), out_shape=(j...]
    all_gather x5 -> x0, waiting for transfers between devices: 73.1 us -> none  [the longest x1 41.2 us: shards(): lax.all_gather(w_gate, 'sp', axis=0, tiled=True)]
    all_gather x2 -> x0, blocking collectives: 65.5 us -> none  [the longest x1 33.8 us: shards(): lax.all_gather(w_value, 'sp', axis=0, tiled=True)]
    reduce_scatter x1 -> x0, waiting for transfers between devices: 43.7 us -> none  [shards(): lax.psum_scatter((jnp.dot(attn_out, attn_weight, preferred_element_type=j...]
    dot_general x7 -> x2, matrix products: 25.7 us -> 3.09 us  [the longest x1 1.88 us: ring_shards(): jnp.einsum('bqkgd,bjkd->bkgqj', query_blk, windows(key_ext), preferred_el...]
    another operation x1 -> x0, loops' own time: 7.56 us -> none  [shards(): lax.map(attend, starts).reshape(token_count, heads_local * HEAD_DIM)]
    reduce_sum x4 -> x2, other arithmetic: 13.1 us -> 7.51 us  [the longest x1 6.46 us: ring_shards(): jnp.sum(conv_sum, axis=1)]
    concatenate x2 -> x4, other arithmetic: 0.03 us -> 4.45 us  [the longest x1 1.69 us: ring_shards(): o_own = jnp.concatenate([out_attn, out_conv], axis=0)]
  transfers between devices with their start and end apart: 9 -> 3, of which waited for: 5 -> 0; matrix products, arithmetic and copies ran while one was open for 17% -> 15% of each run, Pallas kernels for 0% -> 0%
where the time goes in v1:
time: 159 us; the launch traced here: 158 us
  Pallas kernels  97.3 us (61%)
  other arithmetic  24.1 us (15%)
  local copies, waits for them, and re-layouts  16.4 us (10%)
  starting transfers between devices  10.9 us (7%)
  blocking collectives  5.95 us (4%)
  matrix products  3.09 us (2%)
    pallas_call x1, Pallas kernels, gather_and_project(): pl.pallas_call(functools.partial(project_kernel, n, pieces), out_shape=(j...  66.8 us
    pallas_call x1, Pallas kernels, mix_and_scatter(): pl.pallas_call(functools.partial(mix_kernel, parts), out_shape=jax.ShapeD...  30.4 us
    ppermute x3, starting transfers between devices, shifted(): return lax.ppermute(block, axis, route)  10.9 us
    reduce_sum x1, other arithmetic, ring_shards(): jnp.sum(conv_sum, axis=1)  6.46 us
    psum x1, blocking collectives, ring_shards(): lax.psum((jnp.sum(conv_sum, axis=1), jnp.sum(conv_sum * conv_sum, axis=1)...  5.95 us
    unnamed x11, local copies, waits for them, and re-layouts  4.08 us
  transfers between devices with their start and end apart: 3, of which 0 were waited for; matrix products, arithmetic and copies ran while one was open for 15% of the time, Pallas kernels for 0%

profile of v1, /device:TPU:0, one launch (start us, length us, event | category | flops | bytes accessed | tf_op | source)
XLA Modules:
  0.0 157.9 jit_solution(8203650620686125608)
XLA Ops:
  1.8 1.7 %pad_maximum_fusion.5.o_ref = bf16[512,256]{1,0:T(8,128)(2,1)} fusion(bf16[256,256]{1,0:T(8,128)(2,1)} %param.25, bf16[256,256]{1,0:T(8,128)(2,1)} %param.24), kind=kLoop, calls=%fused_computation.103 | loop fusion | flops 524288 | bytes 524288 | tf_op jit(solution)/shard_map/concatenate | solution.py:429
  3.5 1.9 %concatenate.58.w_ref = bf16[256,896]{1,0:T(8,128)(2,1)} concatenate(bf16[256,256]{1,0:T(8,128)(2,1)} %param.15, bf16[256,64]{1,0:T(8,128)(2,1)S(1)} %copy.23, bf16[256,64]{1,0:T(8,128)(2,1)S(1)} %copy.24, bf16[256,256]{1,0:T(8,128)(2,1)} %param.18, bf16[256,256]{1,0:T(8,128)(2,1)} %param.19), dimensions={1} | concatenate | bytes 917504 | tf_op jit(solution)/shard_map/concatenate | solution.py:428
  5.4 66.8 %gather_project.1 = (f32[1024,896]{1,0:T(8,128)}, bf16[8,512,256]{2,1,0:T(8,128)(2,1)}) custom-call(bf16[1024,2048]{1,0:T(8,128)(2,1)} %tok_ref.1, f32[1,2048]{1,0:T(1,128)} %bitcast.102, bf16[256,896]{1,0:T(8,128)(2,1)} %concatenate.58.w_ref, bf16[512,256]{1,0:T(8,128)(2,1)} %pad_maximum_fusion.5.o_ref), custom_call_target="tpu_custom_call" | custom-call | tf_op jit(solution)/shard_map/gather_project/pallas_call | solution.py:151
  72.2 1.2 slice_bitcast_fusion
  73.5 2.4 %fusion.16 = (bf16[1024,1,32]{2,0,1:T(8,128)(2,1)S(1)}, bf16[1024,1,32]{2,0,1:T(8,128)(2,1)S(1)}) fusion(f32[1024,1,64]{2,0,1:T(8,128)S(1)} %slice_bitcast_fusion, f32[32]{0:T(128)S(1)} %negate_power_fusion, f32[1024]{0:T(1024)S(1)} %add_convert_fusion.1), kind=kLoop, calls=%fused_computation.51 | loop fusion | flops 294912 | bytes 397440 | tf_op jit(solution)/shard_map/convert.8
  76.6 4.0 %collective-permute-start.1 = (bf16[128,1,64]{2,0,1:T(8,128)(2,1)}, bf16[128,1,64]{2,0,1:T(8,128)(2,1)}, u32[]{:S(2)}, u32[]{:S(2)}) collective-permute-start(bf16[128,1,64]{2,0,1:T(8,128)(2,1)} %pad_maximum_fusion.6), channel_id=1, source_target_pairs={{0,4},{4,8},{8,12},{12,16},{16,20},{20,24},{24,28},{1,5},{5,9},{9,... | collective-permute-start | bytes 49160 | tf_op jit(solution)/shard_map/ppermute | solution.py:24
  80.6 2.2 %fusion.68 = (f32[1024,256]{1,0:T(8,128)S(1)}, bf16[1024,256]{1,0:T(8,128)(2,1)S(1)}) fusion(f32[1024,896]{1,0:T(8,128)} %get-tuple-element.7), kind=kLoop, calls=%fused_computation.135 | loop fusion | flops 1310720 | bytes 4718592 | tf_op jit(solution)/shard_map/slice | solution.py:436
  83.4 2.8 %collective-permute-start.2 = (bf16[30,256]{1,0:T(8,128)(2,1)}, bf16[30,256]{1,0:T(8,128)(2,1)S(1)}, u32[]{:S(2)}, u32[]{:S(2)}) collective-permute-start(bf16[30,256]{1,0:T(8,128)(2,1)} %slice.327), channel_id=1, source_target_pairs={{0,4},{4,8},{8,12},{12,16},{16,20},{20,24},{24,28},{1,5},{5,9},{9,... | collective-permute-start | bytes 46088 | tf_op jit(solution)/shard_map/ppermute | solution.py:24
  87.1 4.0 %collective-permute-start = (bf16[128,1,64]{2,0,1:T(8,128)(2,1)}, bf16[128,1,64]{2,0,1:T(8,128)(2,1)}, u32[]{:S(2)}, u32[]{:S(2)}) collective-permute-start(bf16[128,1,64]{2,0,1:T(8,128)(2,1)} %slice_bitcast_fusion.1), channel_id=1, source_target_pairs={{0,4},{4,8},{8,12},{12,16},{16,20},{20,24},{24,28},{1,5},{5,9},{9,... | collective-permute-start | bytes 49160 | tf_op jit(solution)/shard_map/ppermute | solution.py:24
  91.1 1.2 multiply_cosine_fusion.1
  95.5 1.8 %broadcast_and_fusion = pred[8,128,256]{1,2,0:T(8,128)(4,1)} fusion(pred[8,256]{1,0:T(8,128)(4,1)} %add_compare_fusion, pred[128,256]{0,1:T(8,128)(4,1)} %fusion.62), kind=kLoop, calls=%fused_computation.95 | loop fusion | flops 262144 | bytes 296960 | tf_op jit(solution)/shard_map/and | solution.py:478
  97.3 1.1 fusion.52
  98.4 0.9 copy_bitcast_fusion
  99.3 1.0 fusion.70
  101.8 1.1 copy.26
  102.9 6.5 %fusion.67 = (f32[1024]{0:T(1024)S(1)}, f32[1024]{0:T(1024)S(1)}, f32[1024,256]{1,0:T(8,128)S(1)}) fusion(bf16[1024,256]{1,0:T(8,128)(2,1)S(1)} %get-tuple-element.15, f32[256]{0:T(256)S(1)} %bitcast.132, bf16[30,256]{1,0:T(8,128)(2,1)S(1)} %collective-permute-done.2, f32[256]{0:T(256)S(1)} %bitcast.133, f32[256]{0:T(256)} %bitcast.104, f32[256]{0:T(256)} %bitcast.105, ...), kind=kLoop, calls=%fused_computation.134 | loop fusion | flops 48756736 | bytes 1629184 | tf_op jit(solution)/shard_map/reduce_sum | solution.py:494
  109.3 6.0 %all-reduce = (f32[1024]{0:T(1024)S(1)}, f32[1024]{0:T(1024)S(1)}) all-reduce(f32[1024]{0:T(1024)S(1)} %get-tuple-element.10, f32[1024]{0:T(1024)S(1)} %get-tuple-element.9), channel_id=1, replica_groups=mesh['sp'=8,'tp'=4] {'tp'}, use_global_device_ids=true, to_apply=%region_5.6 | all-reduce | flops 2048 | bytes 16384 | tf_op jit(solution)/shard_map/psum | solution.py:493
  115.3 1.1 multiply_convert_fusion
  118.4 1.9 %fusion.1 = (f32[8,4,128]{2,1,0:T(4,128)S(1)}, f32[8,256,128,4]{2,1,3,0:T(8,128)S(1)}) fusion(pred[8,128,256]{1,2,0:T(8,128)(4,1)S(1)} %copy-done.1, bf16[8,128,4,32]{1,3,2,0:T(8,128)(2,1)} %get-tuple-element.59, bf16[8,128,4,32]{1,3,2,0:T(8,128)(2,1)} %get-tuple-element.60, bf16[8,128,1,32]{1,3,0,2:T(8,128)(2,1)} %copy.28, ...), kind=kOutput, calls=%fused_computation.33 | convolution fusion | flops 139194368 | bytes 5259264 | tf_op jit(solution)/shard_map/bqkgd,bjkd->bkgqj/dot_general | solution.py:471
  120.4 1.1 fusion
  121.5 1.2 fusion.8
  124.1 1.1 pad_maximum_fusion.act_ref
  125.2 30.4 %mix_scatter.1 = bf16[256,2048]{1,0:T(8,128)(2,1)} custom-call(bf16[1024,512]{1,0:T(8,128)(2,1)} %pad_maximum_fusion.act_ref, bf16[8,512,256]{2,1,0:T(8,128)(2,1)} %get-tuple-element.8.og_ref), custom_call_target="tpu_custom_call" | custom-call | tf_op jit(solution)/shard_map/mix_scatter/pallas_call | solution.py:256
  155.6 2.3 %copy.46 = bf16[256,2048]{1,0:T(8,128)(2,1)} copy(bf16[256,2048]{1,0:T(8,128)(2,1)} %mix_scatter.1) | data formatting | bytes 2097152
  (37 shorter events, 12.2 us)
Async XLA Ops:
  72.2 14.0 %copy-start = (f32[1024,896]{1,0:T(8,128)S(1)}, f32[1024,896]{1,0:T(8,128)}, u32[]{:S(2)}) copy-start(f32[1024,896]{1,0:T(8,128)} %get-tuple-element.7) | copy-start | bytes 11010052
  76.6 39.8 %collective-permute-start.1 = (bf16[128,1,64]{2,0,1:T(8,128)(2,1)}, bf16[128,1,64]{2,0,1:T(8,128)(2,1)}, u32[]{:S(2)}, u32[]{:S(2)}) collective-permute-start(bf16[128,1,64]{2,0,1:T(8,128)(2,1)} %pad_maximum_fusion.6), channel_id=1, source_target_pairs={{0,4},{4,8},{8,12},{12,16},{16,20},{20,24},{24,28},{1,5},{5,9},{9,... | collective-permute-start | bytes 49160 | tf_op jit(solution)/shard_map/ppermute | solution.py:24
  82.7 11.8 %copy-start.2 = (f32[31,256]{1,0:T(8,128)S(1)}, f32[31,256]{1,0:T(8,128)}, u32[]{:S(2)}) copy-start(f32[31,256]{1,0:T(8,128)} %param.21) | copy-start | bytes 95236
  83.4 19.5 %collective-permute-start.2 = (bf16[30,256]{1,0:T(8,128)(2,1)}, bf16[30,256]{1,0:T(8,128)(2,1)S(1)}, u32[]{:S(2)}, u32[]{:S(2)}) collective-permute-start(bf16[30,256]{1,0:T(8,128)(2,1)} %slice.327), channel_id=1, source_target_pairs={{0,4},{4,8},{8,12},{12,16},{16,20},{20,24},{24,28},{1,5},{5,9},{9,... | collective-permute-start | bytes 46088 | tf_op jit(solution)/shard_map/ppermute | solution.py:24
  87.1 30.4 %collective-permute-start = (bf16[128,1,64]{2,0,1:T(8,128)(2,1)}, bf16[128,1,64]{2,0,1:T(8,128)(2,1)}, u32[]{:S(2)}, u32[]{:S(2)}) collective-permute-start(bf16[128,1,64]{2,0,1:T(8,128)(2,1)} %slice_bitcast_fusion.1), channel_id=1, source_target_pairs={{0,4},{4,8},{8,12},{12,16},{16,20},{20,24},{24,28},{1,5},{5,9},{9,... | collective-permute-start | bytes 49160 | tf_op jit(solution)/shard_map/ppermute | solution.py:24
  98.4 20.0 %copy-start.1 = (pred[8,128,256]{1,2,0:T(8,128)(4,1)S(1)}, pred[8,128,256]{1,2,0:T(8,128)(4,1)}, u32[]{:S(2)}) copy-start(pred[8,128,256]{1,2,0:T(8,128)(4,1)} %broadcast_and_fusion) | copy-start | bytes 786436
  116.4 3.9 %copy-start.3 = (f32[4]{0:T(128)S(1)}, f32[4]{0:T(128)}, u32[]{:S(2)}) copy-start(f32[4]{0:T(128)} %param.20) | copy-start | bytes 52

commit v2 on v1

--- a/solution.py
+++ b/solution.py
@@ -59,14 +59,22 @@
 
 
 def project_kernel(
-    n, pieces, tok_ref, gain_ref, w_ref, o_ref, proj_ref, og_ref,
-    scaled, inv, wg, w_send, w_recv, o_send, o_recv,
+    n, pieces, head_lanes,
+    tok_ref, gain_ref, w_ref, o_ref, cos_ref, sin_ref, sink_ref, taps_ref, bias_ref, chan_ref,
+    act_ref, og_ref,
+    scaled, inv, wg, proj_ref, turned, key_ext, value_ext, glu_ext, conv, stats, peer_stats,
+    w_send, w_recv, o_send, o_recv, halo_send, halo_recv, stat_send, stat_recv,
 ):
     me = lax.axis_index("sp")
     place = ring_place(me, n)
     after = {"sp": ring_member(lax.rem(place + 1, n), n)}
     before = {"sp": ring_member(lax.rem(place + n - 1, n), n)}
-    greet((after, before))
+    following = {"sp": lax.rem(me + 1, n)}
+    previous = {"sp": lax.rem(me + n - 1, n)}
+    members = lax.axis_size("tp")
+    mine_tp = lax.axis_index("tp")
+    siblings = [{"tp": lax.rem(mine_tp + k, members)} for k in range(1, members)]
+    greet([after, before, following, previous] + siblings)
 
     def hop(own, held, send, recv, d, c, s):
         half = own.shape[0] // 2
@@ -92,8 +100,6 @@
     lanes = [(d, c) for c in range(pieces) for d in range(2)]
     for d, c in lanes:
         w_hop(d, c, 0).start()
-    for d, c in lanes:
-        o_hop(d, c, 0).start()
 
     token_count, width = tok_ref.shape
     depth = w_ref.shape[0]
@@ -128,45 +134,232 @@
             w_hop(d, c, t).wait_recv()
             if t < n - 2:
                 w_hop(d, c, t + 1).start()
+        if t == max(n - 3, 0):
+            for d, c in lanes:
+                o_hop(d, c, 0).start()
+        ready = [k for k in range(1, n) if max(k, n - k) - 1 == t]
+        if ready:
+            owners = [ring_member(lax.rem(place + n - k, n), n) for k in ready]
+            add([(o, lambda o=o: wg[o]) for o in owners], False, t == n - 2)
+
+    def o_advance(t):
+        if t >= n - 1:
+            return
         for d, c in lanes:
             o_hop(d, c, t).wait_recv()
             if t < n - 2:
                 o_hop(d, c, t + 1).start()
-        ready = [k for k in range(1, n) if max(k, n - k) - 1 == t]
-        if ready:
-            owners = [ring_member(lax.rem(place + n - k, n), n) for k in ready]
-            add([(o, lambda o=o: wg[o]) for o in owners], False, t == n - 2)
+
+    head_w = LANES // 2
+    channels = taps_ref.shape[1]
+    at_glu = head_lanes + LANES
+    lead = glu_ext.shape[0] - token_count
+    tiles = token_count // WINDOW
+
+    def lane_of(shape):
+        return lax.broadcasted_iota(jnp.int32, shape, 1)
+
+    def turn(x, cosine, sine_part):
+        low = lane_of(x.shape) % head_w < head_w // 2
+        swapped = jnp.where(
+            low, pltpu.roll(x, LANES - head_w // 2, 1), pltpu.roll(x, head_w // 2, 1)
+        )
+        return x * cosine + swapped * sine_part
+
+    def shape_rows(i):
+        base = pl.multiple_of(i * WINDOW, WINDOW)
+        rows = pl.ds(base, WINDOW)
+        cosine, sine_part = cos_ref[rows, :], sin_ref[rows, :]
+        for start in range(0, head_lanes, LANES):
+            cut = slice(start, start + LANES)
+            turned[rows, cut] = turn(proj_ref[rows, cut], cosine, sine_part).astype(jnp.bfloat16)
+        pair = proj_ref[rows, head_lanes:at_glu]
+        key_part = turn(pair, cosine, sine_part)
+        low = lane_of(pair.shape) < head_w
+        ext = pl.ds(base + WINDOW, WINDOW)
+        key_ext[ext, :] = jnp.where(low, key_part, pltpu.roll(key_part, head_w, 1)).astype(
+            jnp.bfloat16
+        )
+        value_ext[ext, :] = jnp.where(low, pltpu.roll(pair, head_w, 1), pair).astype(jnp.bfloat16)
+        content = proj_ref[rows, at_glu : at_glu + channels]
+        gate = proj_ref[rows, at_glu + channels : at_glu + 2 * channels]
+        glu_ext[pl.ds(base + lead, WINDOW), :] = (
+            (content * jax.nn.sigmoid(gate)).astype(jnp.bfloat16).astype(jnp.float32)
+        )
+
+    pl.loop(0, tiles)(shape_rows)
+
+    def halo(which):
+        ref, count = ((key_ext, WINDOW), (value_ext, WINDOW), (glu_ext, lead))[which]
+        return pltpu.make_async_remote_copy(
+            src_ref=ref.at[pl.ds(token_count, count)],
+            dst_ref=ref.at[pl.ds(0, count)],
+            send_sem=halo_send.at[which],
+            recv_sem=halo_recv.at[which],
+            device_id=following,
+            device_id_type=MESH,
+        )
+
+    for which in range(3):
+        halo(which).start()
+
+    def convolve(i):
+        base = pl.multiple_of(i * WINDOW, WINDOW)
+        shift = lead - (KERNEL - 1)
+        row_sum = row_squares = None
+        for start in range(0, channels, LANES):
+            cut = slice(start, start + LANES)
+            parts = []
+            for sub in range(0, WINDOW, 64):
+                slab = glu_ext[pl.ds(base + sub, 64 + lead), cut]
+                total = jnp.zeros((64, LANES), jnp.float32) + bias_ref[:, cut]
+                for r in range(8):
+                    moved = slab if r == 0 else pltpu.roll(slab, 64 + lead - r, 0)
+                    for m in range(0, lead + 1, 8):
+                        tap = m + r - shift
+                        if 0 <= tap < KERNEL:
+                            total = total + taps_ref[tap : tap + 1, cut] * moved[m : m + 64]
+                parts.append(total)
+            summed = jnp.concatenate(parts, axis=0)
+            conv[pl.ds(base, WINDOW), cut] = summed
+            one = jnp.sum(summed, axis=1, keepdims=True)
+            two = jnp.sum(summed * summed, axis=1, keepdims=True)
+            row_sum = one if row_sum is None else row_sum + one
+            row_squares = two if row_squares is None else row_squares + two
+        lane = lane_of((WINDOW, LANES))
+        packed = jnp.where(lane == 0, row_sum, jnp.where(lane == 1, row_squares, 0.0))
+        stats[:, pl.ds(base, WINDOW)] = packed.T[:8, :]
+
+    half_tiles = max(tiles // 2, 1)
+    pl.loop(1, half_tiles)(convolve)
+    o_advance(0)
+    pl.loop(half_tiles, tiles)(convolve)
+    halo(2).wait_recv()
+    glu_ext[0:lead, :] = jnp.where(me > 0, glu_ext[0:lead, :], 0.0)
+    convolve(0)
+
+    def stat_copy(k):
+        return pltpu.make_async_remote_copy(
+            src_ref=stats,
+            dst_ref=peer_stats.at[k],
+            send_sem=stat_send.at[k],
+            recv_sem=stat_recv.at[k],
+            device_id=siblings[k],
+            device_id_type=MESH,
+        )
+
+    for k in range(members - 1):
+        stat_copy(k).start()
+    o_advance(1)
+
+    def attend(i):
+        base = pl.multiple_of(i * WINDOW, WINDOW)
+        rows, reach = pl.ds(base, WINDOW), pl.ds(base, 2 * WINDOW)
+        keys, values = key_ext[reach, :], value_ext[reach, :]
+        shape = (WINDOW, 2 * WINDOW)
+        column = lane_of(shape)
+        distance = lax.broadcasted_iota(jnp.int32, shape, 0) - column + WINDOW
+        first = me * token_count + i * WINDOW - WINDOW
+        allowed = (distance >= 0) & (distance < WINDOW) & (column + first >= 0)
+        low = lane_of((WINDOW, LANES)) < head_w
+        for start in range(0, head_lanes, LANES):
+            cut = slice(start, start + LANES)
+            both = turned[rows, cut].astype(jnp.float32)
+            found = []
+            for side in range(2):
+                sink = sink_ref[start // head_w + side]
+                query = jnp.where(low if side == 0 else ~low, both, 0.0).astype(jnp.bfloat16)
+                scores = lax.dot_general(
+                    query, keys, (((1,), (1,)), ((), ())), preferred_element_type=jnp.float32
+                ) * HEAD_DIM ** (-0.5)
+                scores = jnp.where(allowed, scores, -1e30)
+                row_max = jnp.maximum(jnp.max(scores, axis=1, keepdims=True), sink)
+                weights = jnp.exp(scores - row_max)
+                denominator = jnp.sum(weights, axis=1, keepdims=True) + jnp.exp(sink - row_max)
+                probability = (weights * (1.0 / denominator)).astype(jnp.bfloat16)
+                found.append(jnp.dot(probability, values, preferred_element_type=jnp.float32))
+            act_ref[rows, cut] = jnp.where(low, found[0], found[1]).astype(jnp.bfloat16)
+
+    pl.loop(1, half_tiles)(attend)
+    o_advance(2)
+    pl.loop(half_tiles, tiles)(attend)
+    halo(0).wait_recv()
+    halo(1).wait_recv()
+    attend(0)
+    o_advance(3)
+    for k in range(members - 1):
+        stat_copy(k).wait_recv()
+
+    def normalise(i):
+        base = pl.multiple_of(i * WINDOW, WINDOW)
+        rows = pl.ds(base, WINDOW)
+        total = stats[:, rows]
+        for k in range(members - 1):
+            total = total + peer_stats[k, :, rows]
+        total = total * (1.0 / (channels * members))
+        column = jnp.concatenate([total] * (LANES // 8), axis=0).T
+        centre = column[:, 0:1]
+        variance = jnp.maximum(column[:, 1:2] - centre * centre, 0.0)
+        normed = (conv[rows, :] - centre) * lax.rsqrt(variance + EPS) * chan_ref[...]
+        act_ref[rows, head_lanes : head_lanes + channels] = (
+            normed * jax.nn.sigmoid(normed)
+        ).astype(jnp.bfloat16)
+
+    pl.loop(0, tiles)(normalise)
+    for t in range(4, n - 1):
+        o_advance(t)
+    for which in range(3):
+        halo(which).wait_send()
+    for k in range(members - 1):
+        stat_copy(k).wait_send()
     for t in range(n - 1):
         for d, c in lanes:
             w_hop(d, c, t).wait_send()
             o_hop(d, c, t).wait_send()
 
 
-def gather_and_project(n, tokens, gain, w_own, o_own):
+def gather_and_mix(n, tokens, gain, w_own, o_own, cosine, sine_part, sink, taps, bias, chan):
     token_count = tokens.shape[0]
-    width = w_own.shape[1]
+    channels = taps.shape[1]
+    head_lanes = sink.shape[0] * HEAD_DIM
+    lead = -(-(KERNEL - 1) // 8) * 8
+    members = lax.axis_size("tp")
     pieces = 2
-    sems = pltpu.SemaphoreType.DMA((2, n - 1, pieces))
+    dma = pltpu.SemaphoreType.DMA
+    sems = dma((2, n - 1, pieces))
     vmem = pl.BlockSpec(memory_space=pltpu.VMEM)
+    smem = pl.BlockSpec(memory_space=pltpu.SMEM)
     return pl.pallas_call(
-        functools.partial(project_kernel, n, pieces),
+        functools.partial(project_kernel, n, pieces, head_lanes),
         out_shape=(
-            jax.ShapeDtypeStruct((token_count, width), jnp.float32),
+            jax.ShapeDtypeStruct((token_count, head_lanes + channels), jnp.bfloat16),
             jax.ShapeDtypeStruct((n,) + o_own.shape, jnp.bfloat16),
         ),
-        in_specs=[vmem] * 4,
+        in_specs=[vmem] * 6 + [smem] + [vmem] * 3,
         out_specs=(vmem, vmem),
         scratch_shapes=[
             pltpu.VMEM(tokens.shape, jnp.bfloat16),
             pltpu.VMEM((token_count, 1), jnp.float32),
             pltpu.VMEM((n,) + w_own.shape, jnp.bfloat16),
+            pltpu.VMEM((token_count, w_own.shape[1]), jnp.float32),
+            pltpu.VMEM((token_count, head_lanes), jnp.bfloat16),
+            pltpu.VMEM((token_count + WINDOW, LANES), jnp.bfloat16),
+            pltpu.VMEM((token_count + WINDOW, LANES), jnp.bfloat16),
+            pltpu.VMEM((token_count + lead, channels), jnp.float32),
+            pltpu.VMEM((token_count, channels), jnp.float32),
+            pltpu.VMEM((8, token_count), jnp.float32),
+            pltpu.VMEM((members - 1, 8, token_count), jnp.float32),
             sems, sems, sems, sems,
+            dma((3,)), dma((3,)), dma((members - 1,)), dma((members - 1,)),
         ],
         compiler_params=pltpu.CompilerParams(
             collective_id=0, has_side_effects=True, vmem_limit_bytes=VMEM_GRANT
         ),
-        name="gather_project",
-    )(tokens, gain[None, :], w_own, o_own)
+        name="gather_mix",
+    )(
+        tokens, gain[None, :], w_own, o_own, cosine, sine_part, sink, taps,
+        bias[None, :], chan[None, :],
+    )
 
 
 def mix_kernel(
@@ -418,88 +611,19 @@
     token_count = tokens.shape[0]
     offset = lax.axis_index("sp") * token_count
     positions = offset + jnp.arange(token_count, dtype=jnp.int32)
-    widths = [
-        w_query.shape[1],
-        w_key.shape[1],
-        w_value.shape[1],
-        w_content.shape[1],
-        w_gate.shape[1],
-    ]
     w_own = jnp.concatenate([w_query, w_key, w_value, w_content, w_gate], axis=1)
     o_own = jnp.concatenate([out_attn, out_conv], axis=0)
-    projected, mix_weight = gather_and_project(
-        lax.axis_size("sp"), tokens, norm_gain, w_own, o_own
-    )
-    bounds = [0]
-    for width in widths:
-        bounds.append(bounds[-1] + width)
-    proj_query = projected[:, bounds[0] : bounds[1]]
-    proj_key = projected[:, bounds[1] : bounds[2]]
-    proj_value = projected[:, bounds[2] : bounds[3]]
-    proj_content = projected[:, bounds[3] : bounds[4]]
-    proj_gate = projected[:, bounds[4] : bounds[5]]
-    kv_local = widths[1] // HEAD_DIM
-    heads_local = widths[0] // HEAD_DIM
-    group_size = heads_local // kv_local
-    queries = rotate(proj_query.reshape(token_count, heads_local, HEAD_DIM), positions).astype(
-        jnp.bfloat16
-    )
-    key_rows = rotate(proj_key.reshape(token_count, kv_local, HEAD_DIM), positions).astype(
-        jnp.bfloat16
-    )
-    value_rows = proj_value.astype(jnp.bfloat16).reshape(token_count, kv_local, HEAD_DIM)
-    glu_out = (proj_content * jax.nn.sigmoid(proj_gate)).astype(jnp.bfloat16)
-    prior_key, prior_value, prior_glu = shifted(
-        (
-            key_rows[token_count - WINDOW :],
-            value_rows[token_count - WINDOW :],
-            glu_out[token_count - (KERNEL - 1) :],
-        ),
-        "sp",
-        1,
-    )
-    key_ext = jnp.concatenate([prior_key, key_rows], 0)
-    value_ext = jnp.concatenate([prior_value, value_rows], 0)
-    blocks = token_count // WINDOW
-    sink_col = sink_logit.reshape(kv_local, group_size)[None, :, :, None, None]
-    query_blk = queries.reshape(blocks, WINDOW, kv_local, group_size, HEAD_DIM)
-
-    def windows(ext):
-        cut = ext.reshape(blocks + 1, WINDOW, kv_local, HEAD_DIM)
-        return jnp.concatenate([cut[:-1], cut[1:]], axis=1)
-
-    scores = jnp.einsum(
-        "bqkgd,bjkd->bkgqj", query_blk, windows(key_ext), preferred_element_type=jnp.float32
-    ) * HEAD_DIM ** (-0.5)
-    query_off = jnp.arange(WINDOW, dtype=jnp.int32)
-    key_off = jnp.arange(2 * WINDOW, dtype=jnp.int32) - WINDOW
-    distance = query_off[:, None] - key_off[None, :]
-    key_pos = offset + jnp.arange(blocks, dtype=jnp.int32)[:, None] * WINDOW + key_off[None, :]
-    allowed = ((distance >= 0) & (distance < WINDOW))[None] & (key_pos >= 0)[:, None, :]
-    scores = jnp.where(allowed[:, None, None], scores, -1e30)
-    row_max = jnp.maximum(jnp.max(scores, axis=-1, keepdims=True), sink_col)
-    weights = jnp.exp(scores - row_max)
-    denominator = jnp.sum(weights, axis=-1, keepdims=True) + jnp.exp(sink_col - row_max)
-    probability = (weights / denominator).astype(jnp.bfloat16)
-    attended = jnp.einsum(
-        "bkgqj,bjkd->bqkgd", probability, windows(value_ext), preferred_element_type=jnp.float32
-    )
-    attn_out = attended.reshape(token_count, heads_local * HEAD_DIM).astype(jnp.bfloat16)
-    padded = jnp.concatenate([prior_glu, glu_out], 0)
-    conv_sum = jnp.zeros(glu_out.shape, jnp.float32) + conv_bias[None, :]
-    for tap_index in range(KERNEL):
-        window_rows = lax.slice_in_dim(padded, tap_index, tap_index + token_count, axis=0)
-        conv_sum = conv_sum + conv_weight[tap_index][None, :] * window_rows.astype(jnp.float32)
-    row_sum, row_squares = lax.psum(
-        (jnp.sum(conv_sum, axis=1), jnp.sum(conv_sum * conv_sum, axis=1)), "tp"
-    )
-    centre = row_sum / CONV_CH
-    variance = jnp.maximum(row_squares / CONV_CH - centre * centre, 0.0)
-    centred = conv_sum - centre[:, None]
-    conv_out = jax.nn.silu(
-        centred * lax.rsqrt(variance + EPS)[:, None] * channel_gain[None, :]
-    ).astype(jnp.bfloat16)
-    return mix_and_scatter(jnp.concatenate([attn_out, conv_out], axis=1), mix_weight)
+    lane = jnp.arange(LANES, dtype=jnp.int32)
+    half_dim = HEAD_DIM // 2
+    inverse = 1.0 / THETA ** ((lane % half_dim).astype(jnp.float32) * 2.0 / HEAD_DIM)
+    angles = positions.astype(jnp.float32)[:, None] * inverse[None, :]
+    sign = jnp.where(lane % HEAD_DIM < half_dim, -1.0, 1.0)
+    acts, mix_weight = gather_and_mix(
+        lax.axis_size("sp"), tokens, norm_gain, w_own, o_own,
+        jnp.cos(angles), jnp.sin(angles) * sign[None, :],
+        sink_logit, conv_weight, conv_bias, channel_gain,
+    )
+    return mix_and_scatter(acts, mix_weight)
 
 
 def solution(mesh):
@@ -527,6 +651,9 @@
             and arrays[11].shape[1] % LANES == 0
             and arrays[2].shape[0] % LANES == 0
             and arrays[0].shape[0] % (WINDOW * tp) == 0
+            and arrays[2].shape[1] % LANES == 0
+            and arrays[3].shape[1] == HEAD_DIM
+            and arrays[5].shape[1] % LANES == 0
         )
         return (ring_shards if fits else plain_shards)(*arrays)
 

time: 159 us -> 120 us (0.75)
  other arithmetic: 24.1 us -> 4.74 us
  Pallas kernels: 97.3 us -> 109 us
  starting transfers between devices: 10.9 us -> 0 us
  local copies, waits for them, and re-layouts: 16.4 us -> 5.99 us
  blocking collectives: 5.95 us -> 0 us
  matrix products: 3.09 us -> 0 us
    pallas_call x1, Pallas kernels: 66.8 us -> 79.1 us  [gather_and_mix(): pl.pallas_call(functools.partial(project_kernel, n, pieces, head_lanes),...]
    ppermute x3 -> x0, starting transfers between devices: 10.9 us -> none  [shifted(): return lax.ppermute(block, axis, route)]
    reduce_sum x2 -> x0, other arithmetic: 7.51 us -> none  [the longest x1 6.46 us: ring_shards(): jnp.sum(conv_sum, axis=1)]
    psum x1 -> x0, blocking collectives: 5.95 us -> none  [ring_shards(): lax.psum((jnp.sum(conv_sum, axis=1), jnp.sum(conv_sum * conv_sum, axis=1)...]
    slice x8 -> x0, local copies, waits for them, and re-layouts: 4.61 us -> none  [the longest x2 1.63 us: ring_shards(): conv_weight[tap_index][None, :] * window_rows.astype(jnp.float32)]
    concatenate x4 -> x0, other arithmetic: 3.45 us -> none  [the longest x1 1.05 us: ring_shards(): jnp.concatenate([attn_out, conv_out], axis=1)]
    dot_general x2 -> x0, matrix products: 3.09 us -> none  [the longest x1 1.88 us: ring_shards(): jnp.einsum('bqkgd,bjkd->bkgqj', query_blk, windows(key_ext), preferred_el...]
    mul x0 -> x1, other arithmetic: none -> 3.04 us  [ring_shards(): jnp.sin(angles) * sign[None, :]]
  transfers between devices with their start and end apart: 3 -> 0, of which waited for: 0 -> 0; matrix products, arithmetic and copies ran while one was open for 15% -> 0% of each run, Pallas kernels for 0% -> 0%
where the time goes in v2:
time: 120 us
  Pallas kernels  109 us (91%)
  local copies, waits for them, and re-layouts  5.99 us (5%)
  other arithmetic  4.74 us (4%)
    pallas_call x1, Pallas kernels, gather_and_mix(): pl.pallas_call(functools.partial(project_kernel, n, pieces, head_lanes),...  79.1 us
    pallas_call x1, Pallas kernels, mix_and_scatter(): pl.pallas_call(functools.partial(mix_kernel, parts), out_shape=jax.ShapeD...  30 us
    unnamed x3, local copies, waits for them, and re-layouts  4.06 us
    mul x1, other arithmetic, ring_shards(): jnp.sin(angles) * sign[None, :]  3.04 us

profile of v2, /device:TPU:0, one launch (start us, length us, event | category | flops | bytes accessed | tf_op | source)
XLA Modules:
  0.0 119.8 jit_solution(13839340373265949808)
XLA Ops:
  0.0 0.9 copy.14
  0.9 0.9 copy.15
  1.8 1.7 %pad_maximum_fusion.o_ref = bf16[512,256]{1,0:T(8,128)(2,1)} fusion(bf16[256,256]{1,0:T(8,128)(2,1)} %param.25, bf16[256,256]{1,0:T(8,128)(2,1)} %param.24), kind=kLoop, calls=%fused_computation.3 | loop fusion | flops 524288 | bytes 524288 | tf_op jit(solution)/shard_map/concatenate | solution.py:615
  3.5 1.9 %concatenate.6.w_ref = bf16[256,896]{1,0:T(8,128)(2,1)} concatenate(bf16[256,256]{1,0:T(8,128)(2,1)} %param.15, bf16[256,64]{1,0:T(8,128)(2,1)S(1)} %copy.14, bf16[256,64]{1,0:T(8,128)(2,1)S(1)} %copy.15, bf16[256,256]{1,0:T(8,128)(2,1)} %param.18, bf16[256,256]{1,0:T(8,128)(2,1)} %param.19), dimensions={1} | concatenate | bytes 917504 | tf_op jit(solution)/shard_map/concatenate | solution.py:614
  5.4 3.0 %fusion = (f32[1024,128]{1,0:T(8,128)}, f32[1024,128]{1,0:T(8,128)}) fusion(f32[128]{0:T(128)S(1)} %get-tuple-element.11, f32[128]{0:T(128)S(1)} %get-tuple-element.12, f32[1024]{0:T(1024)S(1)} %add_convert_fusion), kind=kLoop, calls=%fused_computation.2 | loop fusion | flops 262144 | bytes 1053696 | tf_op jit(solution)/shard_map/mul | solution.py:623
  8.4 79.1 %gather_mix.1 = (bf16[1024,512]{1,0:T(8,128)(2,1)}, bf16[8,512,256]{2,1,0:T(8,128)(2,1)}) custom-call(bf16[1024,2048]{1,0:T(8,128)(2,1)} %tok_ref.1, f32[1,2048]{1,0:T(1,128)} %bitcast.3, bf16[256,896]{1,0:T(8,128)(2,1)} %concatenate.6.w_ref, bf16[512,256]{1,0:T(8,128)(2,1)} %pad_maximum_fusion.o_ref, f32[1024,128]{1,0:T(8,128)} %get-tuple-element.10.cos_ref, ...), custom_call_target="tpu_custom_call" | custom-call | tf_op jit(solution)/shard_map/gather_mix/pallas_call | solution.py:332
  87.6 30.0 %mix_scatter.1 = bf16[256,2048]{1,0:T(8,128)(2,1)} custom-call(bf16[1024,512]{1,0:T(8,128)(2,1)} %get-tuple-element.7.act_ref, bf16[8,512,256]{2,1,0:T(8,128)(2,1)} %get-tuple-element.8.og_ref), custom_call_target="tpu_custom_call" | custom-call | tf_op jit(solution)/shard_map/mix_scatter/pallas_call | solution.py:449
  117.5 2.3 %copy.17 = bf16[256,2048]{1,0:T(8,128)(2,1)} copy(bf16[256,2048]{1,0:T(8,128)(2,1)} %mix_scatter.1) | data formatting | bytes 2097152
  (2 shorter events, 0.0 us)

commit v3 on v2

--- a/solution.py
+++ b/solution.py
@@ -60,10 +60,12 @@
 
 def project_kernel(
     n, pieces, head_lanes,
-    tok_ref, gain_ref, w_ref, o_ref, cos_ref, sin_ref, sink_ref, taps_ref, bias_ref, chan_ref,
-    act_ref, og_ref,
+    tok_ref, gain_ref, w_ref, oa_ref, oc_ref, cos_ref, sin_ref, far_cos_ref, far_sin_ref,
+    sink_ref, taps_ref, bias_ref, chan_ref, out_ref, act_ref, og_ref,
+    near_out, near_in, far_out, far_in,
     scaled, inv, wg, proj_ref, turned, key_ext, value_ext, glu_ext, conv, stats, peer_stats,
     w_send, w_recv, o_send, o_recv, halo_send, halo_recv, stat_send, stat_recv,
+    near_send, near_recv, far_send, far_recv,
 ):
     me = lax.axis_index("sp")
     place = ring_place(me, n)
@@ -76,14 +78,14 @@
     siblings = [{"tp": lax.rem(mine_tp + k, members)} for k in range(1, members)]
     greet([after, before, following, previous] + siblings)
 
-    def hop(own, held, send, recv, d, c, s):
-        half = own.shape[0] // 2
+    def hop(own, own_start, held, send, recv, d, c, s):
+        half = held.shape[1] // 2
         sub = half // pieces
         rows = pl.ds(d * half + c * sub, sub)
         offset = n - s if d == 0 else s
         owner = ring_member(lax.rem(place + offset, n), n)
         return pltpu.make_async_remote_copy(
-            src_ref=own.at[rows] if s == 0 else held.at[owner, rows],
+            src_ref=own.at[pl.ds(own_start + c * sub, sub)] if s == 0 else held.at[owner, rows],
             dst_ref=held.at[owner, rows],
             send_sem=send.at[d, s, c],
             recv_sem=recv.at[d, s, c],
@@ -92,10 +94,10 @@
         )
 
     def w_hop(d, c, s):
-        return hop(w_ref, wg, w_send, w_recv, d, c, s)
+        return hop(w_ref, d * (w_ref.shape[0] // 2), wg, w_send, w_recv, d, c, s)
 
     def o_hop(d, c, s):
-        return hop(o_ref, og_ref, o_send, o_recv, d, c, s)
+        return hop(oc_ref if d else oa_ref, 0, og_ref, o_send, o_recv, d, c, s)
 
     lanes = [(d, c) for c in range(pieces) for d in range(2)]
     for d, c in lanes:
@@ -113,7 +115,9 @@
         scaled[rows, :] = (wide * gain_ref[...]).astype(jnp.bfloat16)
 
     tile = math.gcd(token_count, 256)
-    og_ref[me] = o_ref[...]
+    attn_rows = oa_ref.shape[0]
+    og_ref[me, 0:attn_rows] = oa_ref[...]
+    og_ref[me, attn_rows:] = oc_ref[...]
 
     def add(terms, first, last):
         @pl.loop(0, token_count // tile)
@@ -164,12 +168,15 @@
         swapped = jnp.where(
             low, pltpu.roll(x, LANES - head_w // 2, 1), pltpu.roll(x, head_w // 2, 1)
         )
-        return x * cosine + swapped * sine_part
+        return x * cosine + jnp.where(low, -swapped, swapped) * sine_part
 
     def shape_rows(i):
         base = pl.multiple_of(i * WINDOW, WINDOW)
         rows = pl.ds(base, WINDOW)
-        cosine, sine_part = cos_ref[rows, :], sin_ref[rows, :]
+        near_cos, near_sin = cos_ref[...], sin_ref[...]
+        far_cos, far_sin = far_cos_ref[pl.ds(i, 1), :], far_sin_ref[pl.ds(i, 1), :]
+        cosine = near_cos * far_cos - near_sin * far_sin
+        sine_part = near_sin * far_cos + near_cos * far_sin
         for start in range(0, head_lanes, LANES):
             cut = slice(start, start + LANES)
             turned[rows, cut] = turn(proj_ref[rows, cut], cosine, sine_part).astype(jnp.bfloat16)
@@ -306,8 +313,75 @@
         ).astype(jnp.bfloat16)
 
     pl.loop(0, tiles)(normalise)
-    for t in range(4, n - 1):
-        o_advance(t)
+
+    near = mine_tp + 1 - 2 * (mine_tp % 2)
+    far = lax.rem(mine_tp + 2, members)
+    far_near = lax.rem(near + 2, members)
+    rows_out = out_ref.shape[0]
+    cols = oa_ref.shape[1]
+
+    def partial_of(member, owner):
+        rows = pl.ds(pl.multiple_of(member * rows_out, rows_out), rows_out)
+        return jnp.dot(act_ref[rows, :], og_ref[owner], preferred_element_type=jnp.float32)
+
+    def near_copy(which, q):
+        return pltpu.make_async_remote_copy(
+            src_ref=near_out.at[which, q],
+            dst_ref=near_in.at[which, q],
+            send_sem=near_send.at[which, q],
+            recv_sem=near_recv.at[which, q],
+            device_id={"tp": near},
+            device_id_type=MESH,
+        )
+
+    def far_copy(q):
+        return pltpu.make_async_remote_copy(
+            src_ref=far_out.at[q],
+            dst_ref=far_in.at[q],
+            send_sem=far_send.at[q],
+            recv_sem=far_recv.at[q],
+            device_id={"tp": far},
+            device_id_type=MESH,
+        )
+
+    distances = [(0, 0)] + sorted((max(k, n - k), k) for k in range(1, n))
+    owners = [ring_member(lax.rem(place + n - k, n), n) for _, k in distances]
+
+    def give_near(which, member, q):
+        near_out[which, q] = partial_of(member, owners[q]).astype(jnp.bfloat16)
+        near_copy(which, q).start()
+
+    def give_far(q):
+        mine = partial_of(far, owners[q])
+        near_copy(0, q).wait_recv()
+        far_out[q] = (mine + near_in[0, q].astype(jnp.float32)).astype(jnp.bfloat16)
+        far_copy(q).start()
+
+    advanced = 4
+    for q in range(n):
+        waits = advanced < distances[q][0]
+        if q > 0 and waits:
+            give_far(q - 1)
+        while advanced < distances[q][0]:
+            o_advance(advanced)
+            advanced += 1
+        give_near(0, far_near, q)
+        if q > 0 and not waits:
+            give_far(q - 1)
+    give_far(n - 1)
+    for q in range(n):
+        give_near(1, near, q)
+    for q in range(n):
+        mine = partial_of(mine_tp, owners[q])
+        near_copy(1, q).wait_recv()
+        mine = mine + near_in[1, q].astype(jnp.float32)
+        far_copy(q).wait_recv()
+        span = pl.ds(pl.multiple_of(owners[q] * cols, cols), cols)
+        out_ref[:, span] = (mine + far_in[q].astype(jnp.float32)).astype(jnp.bfloat16)
+    for q in range(n):
+        near_copy(0, q).wait_send()
+        near_copy(1, q).wait_send()
+        far_copy(q).wait_send()
     for which in range(3):
         halo(which).wait_send()
     for k in range(members - 1):
@@ -318,26 +392,31 @@
             o_hop(d, c, t).wait_send()
 
 
-def gather_and_mix(n, tokens, gain, w_own, o_own, cosine, sine_part, sink, taps, bias, chan):
+def whole_layer(n, tokens, gain, w_own, oa, oc, tables, sink, taps, bias, chan):
     token_count = tokens.shape[0]
     channels = taps.shape[1]
     head_lanes = sink.shape[0] * HEAD_DIM
     lead = -(-(KERNEL - 1) // 8) * 8
     members = lax.axis_size("tp")
     pieces = 2
+    cols = oa.shape[1]
+    rows_out = token_count // members
     dma = pltpu.SemaphoreType.DMA
     sems = dma((2, n - 1, pieces))
     vmem = pl.BlockSpec(memory_space=pltpu.VMEM)
     smem = pl.BlockSpec(memory_space=pltpu.SMEM)
     return pl.pallas_call(
         functools.partial(project_kernel, n, pieces, head_lanes),
-        out_shape=(
-            jax.ShapeDtypeStruct((token_count, head_lanes + channels), jnp.bfloat16),
-            jax.ShapeDtypeStruct((n,) + o_own.shape, jnp.bfloat16),
-        ),
-        in_specs=[vmem] * 6 + [smem] + [vmem] * 3,
-        out_specs=(vmem, vmem),
+        out_shape=jax.ShapeDtypeStruct((rows_out, n * cols), jnp.bfloat16),
+        in_specs=[vmem] * 9 + [smem] + [vmem] * 3,
+        out_specs=vmem,
         scratch_shapes=[
+            pltpu.VMEM((token_count, head_lanes + channels), jnp.bfloat16),
+            pltpu.VMEM((n, oa.shape[0] + oc.shape[0], cols), jnp.bfloat16),
+            pltpu.VMEM((2, n, rows_out, cols), jnp.bfloat16),
+            pltpu.VMEM((2, n, rows_out, cols), jnp.bfloat16),
+            pltpu.VMEM((n, rows_out, cols), jnp.bfloat16),
+            pltpu.VMEM((n, rows_out, cols), jnp.bfloat16),
             pltpu.VMEM(tokens.shape, jnp.bfloat16),
             pltpu.VMEM((token_count, 1), jnp.float32),
             pltpu.VMEM((n,) + w_own.shape, jnp.bfloat16),
@@ -351,121 +430,16 @@
             pltpu.VMEM((members - 1, 8, token_count), jnp.float32),
             sems, sems, sems, sems,
             dma((3,)), dma((3,)), dma((members - 1,)), dma((members - 1,)),
+            dma((2, n)), dma((2, n)), dma((n,)), dma((n,)),
         ],
         compiler_params=pltpu.CompilerParams(
             collective_id=0, has_side_effects=True, vmem_limit_bytes=VMEM_GRANT
         ),
-        name="gather_mix",
+        name="whole_layer",
     )(
-        tokens, gain[None, :], w_own, o_own, cosine, sine_part, sink, taps,
+        tokens, gain[None, :], w_own, oa, oc, *tables, sink, taps,
         bias[None, :], chan[None, :],
     )
-
-
-def mix_kernel(
-    parts, act_ref, og_ref, out_ref, near_out, near_in, far_out, far_in,
-    near_send, near_recv, far_send, far_recv,
-):
-    me = lax.axis_index("tp")
-    core = me % 2
-    near = me + 1 - 2 * core
-    far = lax.rem(me + 2, 4)
-    far_near = lax.rem(near + 2, 4)
-    near_id, far_id = {"tp": near}, {"tp": far}
-    greet((near_id, far_id))
-    rows_out = out_ref.shape[0]
-    blocks = og_ref.shape[0] // parts
-    cols = og_ref.shape[2]
-
-    def partial_of(member, q):
-        rows = pl.ds(pl.multiple_of(member * rows_out, rows_out), rows_out)
-        acts = act_ref[rows, :]
-        return jnp.concatenate(
-            [
-                jnp.dot(acts, og_ref[q * blocks + b], preferred_element_type=jnp.float32)
-                for b in range(blocks)
-            ],
-            axis=1,
-        )
-
-    def near_copy(which, q):
-        return pltpu.make_async_remote_copy(
-            src_ref=near_out.at[which, q],
-            dst_ref=near_in.at[which, q],
-            send_sem=near_send.at[which, q],
-            recv_sem=near_recv.at[which, q],
-            device_id=near_id,
-            device_id_type=MESH,
-        )
-
-    def far_copy(q):
-        return pltpu.make_async_remote_copy(
-            src_ref=far_out.at[q],
-            dst_ref=far_in.at[q],
-            send_sem=far_send.at[q],
-            recv_sem=far_recv.at[q],
-            device_id=far_id,
-            device_id_type=MESH,
-        )
-
-    def give_near(which, member, q):
-        near_out[which, q] = partial_of(member, q).astype(jnp.bfloat16)
-        near_copy(which, q).start()
-
-    def give_far(q):
-        mine = partial_of(far, q)
-        near_copy(0, q).wait_recv()
-        far_out[q] = (mine + near_in[0, q].astype(jnp.float32)).astype(jnp.bfloat16)
-        far_copy(q).start()
-
-    give_near(0, far_near, 0)
-    for q in range(1, parts):
-        give_near(0, far_near, q)
-        give_far(q - 1)
-    give_far(parts - 1)
-    for q in range(parts):
-        give_near(1, near, q)
-    for q in range(parts):
-        mine = partial_of(me, q)
-        near_copy(1, q).wait_recv()
-        mine = mine + near_in[1, q].astype(jnp.float32)
-        far_copy(q).wait_recv()
-        span = blocks * cols
-        out_ref[:, q * span : (q + 1) * span] = (
-            mine + far_in[q].astype(jnp.float32)
-        ).astype(jnp.bfloat16)
-    for q in range(parts):
-        near_copy(0, q).wait_send()
-        near_copy(1, q).wait_send()
-        far_copy(q).wait_send()
-
-
-def mix_and_scatter(acts, og):
-    n, _, cols = og.shape
-    parts = math.gcd(n, 4)
-    rows_out = acts.shape[0] // 4
-    span = n // parts * cols
-    vmem = pl.BlockSpec(memory_space=pltpu.VMEM)
-    return pl.pallas_call(
-        functools.partial(mix_kernel, parts),
-        out_shape=jax.ShapeDtypeStruct((rows_out, n * cols), jnp.bfloat16),
-        in_specs=[vmem] * 2,
-        out_specs=vmem,
-        scratch_shapes=[
-            pltpu.VMEM((2, parts, rows_out, span), jnp.bfloat16),
-            pltpu.VMEM((2, parts, rows_out, span), jnp.bfloat16),
-            pltpu.VMEM((parts, rows_out, span), jnp.bfloat16),
-            pltpu.VMEM((parts, rows_out, span), jnp.bfloat16),
-            pltpu.SemaphoreType.DMA((2, parts)),
-            pltpu.SemaphoreType.DMA((2, parts)),
-            pltpu.SemaphoreType.DMA((parts,)),
-            pltpu.SemaphoreType.DMA((parts,)),
-        ],
-        compiler_params=pltpu.CompilerParams(
-            collective_id=1, has_side_effects=True, vmem_limit_bytes=VMEM_GRANT
-        ),
-        name="mix_scatter",
-    )(acts, og)
 
 
 def plain_shards(
@@ -612,18 +586,16 @@
     offset = lax.axis_index("sp") * token_count
     positions = offset + jnp.arange(token_count, dtype=jnp.int32)
     w_own = jnp.concatenate([w_query, w_key, w_value, w_content, w_gate], axis=1)
-    o_own = jnp.concatenate([out_attn, out_conv], axis=0)
+    half_dim = HEAD_DIM // 2
     lane = jnp.arange(LANES, dtype=jnp.int32)
-    half_dim = HEAD_DIM // 2
     inverse = 1.0 / THETA ** ((lane % half_dim).astype(jnp.float32) * 2.0 / HEAD_DIM)
-    angles = positions.astype(jnp.float32)[:, None] * inverse[None, :]
-    sign = jnp.where(lane % HEAD_DIM < half_dim, -1.0, 1.0)
-    acts, mix_weight = gather_and_mix(
-        lax.axis_size("sp"), tokens, norm_gain, w_own, o_own,
-        jnp.cos(angles), jnp.sin(angles) * sign[None, :],
+    near_angle = jnp.arange(WINDOW, dtype=jnp.float32)[:, None] * inverse[None, :]
+    far_angle = positions[::WINDOW].astype(jnp.float32)[:, None] * inverse[None, :]
+    tables = (jnp.cos(near_angle), jnp.sin(near_angle), jnp.cos(far_angle), jnp.sin(far_angle))
+    return whole_layer(
+        lax.axis_size("sp"), tokens, norm_gain, w_own, out_attn, out_conv, tables,
         sink_logit, conv_weight, conv_bias, channel_gain,
     )
-    return mix_and_scatter(acts, mix_weight)
 
 
 def solution(mesh):
@@ -643,7 +615,7 @@
         P("tp", "sp"),
     )
     sp, tp = mesh.shape["sp"], mesh.shape["tp"]
-    ringed = tp == 4 and sp % 2 == 0
+    ringed = tp == 4 and sp % 2 == 0 and sp >= 6
 
     def shards(*arrays):
         fits = (
@@ -653,6 +625,7 @@
             and arrays[0].shape[0] % (WINDOW * tp) == 0
             and arrays[2].shape[1] % LANES == 0
             and arrays[3].shape[1] == HEAD_DIM
+            and arrays[11].shape[0] == arrays[12].shape[0]
             and arrays[5].shape[1] % LANES == 0
         )
         return (ring_shards if fits else plain_shards)(*arrays)

time: 120 us -> 103 us (0.86)
  Pallas kernels: 109 us -> 94.7 us
  other arithmetic: 4.74 us -> 1.65 us
    pallas_call x2 -> x1, Pallas kernels: 109 us -> 94.7 us  [whole_layer(): pl.pallas_call(functools.partial(project_kernel, n, pieces, head_lanes),...]
    mul x1 -> x0, other arithmetic: 3.04 us -> none  [ring_shards(): jnp.sin(angles) * sign[None, :]]
    concatenate x1 -> x0, other arithmetic: 1.68 us -> none  [ring_shards(): o_own = jnp.concatenate([out_attn, out_conv], axis=0)]
    sin x0 -> x2, other arithmetic: none -> 1.63 us  [the longest x1 0.91 us: ring_shards(): jnp.sin(near_angle)]
where the time goes in v3:
time: 103 us; the launch traced here: 102 us
  Pallas kernels  94.7 us (92%)
  local copies, waits for them, and re-layouts  6.05 us (6%)
  other arithmetic  1.65 us (2%)
    pallas_call x1, Pallas kernels, whole_layer(): pl.pallas_call(functools.partial(project_kernel, n, pieces, head_lanes),...  94.7 us
    unnamed x3, local copies, waits for them, and re-layouts  4.05 us

profile of v3, /device:TPU:0, one launch (start us, length us, event | category | flops | bytes accessed | tf_op | source)
XLA Modules:
  0.0 102.4 jit_solution(17238592412604581909)
XLA Ops:
  0.0 0.1 slice.3
  0.1 0.7 multiply_sine_fusion
  0.8 0.9 copy.14
  1.7 0.9 copy.15
  2.6 0.9 fusion
  3.5 1.9 %concatenate.3.w_ref = bf16[256,896]{1,0:T(8,128)(2,1)} concatenate(bf16[256,256]{1,0:T(8,128)(2,1)} %param.15, bf16[256,64]{1,0:T(8,128)(2,1)S(1)} %copy.14, bf16[256,64]{1,0:T(8,128)(2,1)S(1)} %copy.15, bf16[256,256]{1,0:T(8,128)(2,1)} %param.18, bf16[256,256]{1,0:T(8,128)(2,1)} %param.19), dimensions={1} | concatenate | bytes 917504 | tf_op jit(solution)/shard_map/concatenate | solution.py:588
  5.4 94.7 %whole_layer.1 = bf16[256,2048]{1,0:T(8,128)(2,1)} custom-call(bf16[1024,2048]{1,0:T(8,128)(2,1)} %tok_ref.1, f32[1,2048]{1,0:T(1,128)} %bitcast.3, bf16[256,896]{1,0:T(8,128)(2,1)} %concatenate.3.w_ref, bf16[256,256]{1,0:T(8,128)(2,1)} %oa_ref.1, bf16[256,256]{1,0:T(8,128)(2,1)} %oc_ref.1, f32[128,128]{1,0:T(8,128)} %get-tuple-element.8.cos_ref, ...), custom_call_target="tpu_custom_call" | custom-call | tf_op jit(solution)/shard_map/whole_layer/pallas_call | solution.py:408
  100.1 2.3 %copy.17 = bf16[256,2048]{1,0:T(8,128)(2,1)} copy(bf16[256,2048]{1,0:T(8,128)(2,1)} %whole_layer.1) | data formatting | bytes 2097152
  (3 shorter events, 0.0 us)
